TPU v7x, 32 devices: a whole 2x2x4 slice. The times are simulated.
32 devices in a mesh: sp: 8 (over z, core), tp: 4 (over y, x).
Axes of the slice: x: 2, y: 2, z: 4, core: 2. Of those that a mesh axis runs over, the one named last changes fastest.
Arguments:
- tokens: bfloat16 [2, 6144, 4096], P(None, 'sp', 'tp'), may hold values from -6 to 6
- w_key: bfloat16 [4096, 2048], P(None, 'tp'), may hold values from -0.09375 to 0.09375
- w_value: bfloat16 [4096, 2048], P(None, 'tp'), may hold values from -0.09375 to 0.09375
- w_gate: bfloat16 [4096, 4, 16], replicated, may hold values from -0.09375 to 0.09375
- forget_bias: float32 [2, 16], replicated, may hold values from 3.9 to 13, as said below
- log_shift: float32 [2, 4, 16, 6144], P(None, None, 'tp', 'sp'), may hold values from -5 to 121, as said below
- new_query: bfloat16 [2, 1024, 2048], P(None, 'sp', 'tp'), may hold values from -6 to 6
Outputs:
- cache_matrix: bfloat16 [2, 2, 16, 128, 128], P(None, None, 'tp')
- cache_norm: float32 [2, 2, 16, 128], P(None, None, 'tp')
- cache_max: float32 [2, 2, 16], P(None, None, 'tp')
- first_read: bfloat16 [2, 1024, 2048], P(None, 'sp', 'tp')
Inputs may be any that keep to these rules, and one draw needn't show every extreme that they name: `forget_bias`: added to the forget gates' pre-activations, by direction and head. `log_shift`: rows 0 and 2 are added to the input gates of the two directions; rows 1 and 3 are added to the log forget gates and are never positive.
All inputs are finite; a program needn't handle non-finite values.
Results may differ from a plain program's by a relative error of at most 0.024.
Values may be sent and summed in bfloat16 or wider, within the bound.
No kernel may reach another device: no remote copies, remote signals or barrier semaphores. Data moves between devices by JAX's collectives and lax.ppermute only.
A program may use at most 64 MiB of HBM per device.

v0:
```python
import functools

import jax
import jax.numpy as jnp
from jax import lax
from jax.experimental import pallas as pl
from jax.experimental.pallas import tpu as pltpu
from jax.sharding import PartitionSpec as P


HEAD = 128
SLAB = HEAD + 8


def combined_all(array, axis, combine):
    everything = jax.tree.map(lambda part: lax.all_gather(part, axis), array)
    leading = jax.tree.map(lambda part: part[0], everything)

    def lap(k, so_far):
        return combine(so_far, jax.tree.map(lambda part: part[k], everything))

    return lax.fori_loop(1, lax.axis_size(axis), lap, leading)


def joint_max(earlier, latter):
    memory_a, norm_a, high_a = earlier
    memory_b, norm_b, high_b = latter
    highest = jnp.maximum(high_a, high_b)
    carried = jnp.exp(high_a - highest)
    own_part = jnp.exp(high_b - highest)
    memory = memory_a * carried[..., None, None] + memory_b * own_part[..., None, None]
    norm_sum = norm_a * carried[..., None] + norm_b * own_part[..., None]
    return (memory, norm_sum, highest)


def any_mesh(tokens, w_key, w_value, w_gate, forget_bias, log_shift, new_query):
    seq_count, seg_len, _ = tokens.shape
    per_head = w_key.shape[1] // HEAD
    row_count = seq_count * seg_len
    first_head = lax.axis_index("tp") * per_head
    gate_cols = lax.dynamic_slice_in_dim(w_gate, first_head, per_head, 2).reshape(
        w_gate.shape[0], 4 * per_head
    )
    bias_own = lax.dynamic_slice_in_dim(forget_bias, first_head, per_head, 1)
    piece = lax.all_gather(tokens, "tp", axis=2, tiled=True)
    piece_width = piece.shape[2]
    flat_piece = piece.reshape(row_count, piece_width)
    key_sum = jnp.dot(flat_piece, w_key, preferred_element_type=jnp.float32)
    value_sum = jnp.dot(flat_piece, w_value, preferred_element_type=jnp.float32)
    gate_sum = jnp.dot(flat_piece, gate_cols, preferred_element_type=jnp.float32)
    key_rows = key_sum.astype(jnp.bfloat16).reshape(seq_count, seg_len, per_head, HEAD)
    value_rows = value_sum.astype(jnp.bfloat16).reshape(seq_count, seg_len, per_head, HEAD)
    gates = gate_sum.reshape(seq_count, seg_len, 4, per_head).transpose(0, 2, 3, 1)
    weights, totals = decay(gates, bias_own, log_shift)
    local_top = jnp.max(weights, axis=-1)
    scale_now = jnp.exp(weights - local_top[..., None])
    key_f = key_rows.astype(jnp.float32).transpose(0, 2, 1, 3) * HEAD ** (-0.5)
    value_f = value_rows.astype(jnp.float32).transpose(0, 2, 1, 3)
    weighted = scale_now[..., None] * key_f[:, None]
    memory = jnp.einsum("bjhld,bhle->bjhde", weighted, value_f, precision=lax.Precision.HIGHEST)
    norm_sum = jnp.sum(weighted, axis=3)
    every_total = lax.all_gather(totals[None], "sp", axis=0, tiled=True)
    my_index = lax.axis_index("sp")
    sources = jnp.arange(every_total.shape[0])[:, None, None, None]
    direction = jnp.arange(2)[None, None, :, None]
    counted = jnp.where(direction == 0, sources > my_index, sources < my_index)
    passed = jnp.sum(jnp.where(counted, every_total, 0.0), axis=0)
    total_all = jnp.sum(every_total, axis=0)
    memory_all, norm_all, top_all = combined_all(
        (memory, norm_sum, local_top + passed), "sp", joint_max
    )
    cache_max = jnp.maximum(total_all, top_all)
    rescale = jnp.exp(top_all - cache_max)
    cache_matrix = (memory_all * rescale[..., None, None]).astype(jnp.bfloat16)
    cache_norm = norm_all * rescale[..., None]
    new_count = new_query.shape[1]
    queries = new_query.reshape(seq_count, new_count, per_head, HEAD)
    numerator = jnp.einsum(
        "bthd,bjhde->bjthe", queries, cache_matrix, preferred_element_type=jnp.float32
    )
    denominator = jnp.einsum(
        "bthd,bjhd->bjth", queries.astype(jnp.float32), cache_norm, precision=lax.Precision.HIGHEST
    )
    divisor = jnp.maximum(jnp.abs(denominator), 1.0)
    first_read = jnp.sum(numerator / divisor[..., None], axis=1)
    first_read = first_read.reshape(seq_count, new_count, per_head * HEAD).astype(jnp.bfloat16)
    return (cache_matrix, cache_norm, cache_max, first_read)


def decay(gates, bias_own, log_shift):
    input_fwd = gates[:, 0] + log_shift[:, 0]
    forget_fwd = jax.nn.log_sigmoid(gates[:, 1] + bias_own[0][None, :, None]) + log_shift[:, 1]
    input_bwd = gates[:, 2] + log_shift[:, 2]
    forget_bwd = jax.nn.log_sigmoid(gates[:, 3] + bias_own[1][None, :, None]) + log_shift[:, 3]
    climb = jnp.cumsum(jnp.stack([forget_fwd, forget_bwd], axis=1), axis=-1)
    totals = climb[..., -1]
    weight_fwd = totals[:, 0, :, None] - climb[:, 0] + input_fwd
    weight_bwd = climb[:, 1] - forget_bwd + input_bwd
    return jnp.stack([weight_fwd, weight_bwd], axis=1), totals


def swap(array, axis, bit):
    size = lax.axis_size(axis)
    return lax.ppermute(array, axis, [(i, i ^ bit) for i in range(size)])


def head_weights(w_key, w_value, block, width, h):
    rows = pl.ds(pl.multiple_of(block * width, width), width)
    cols = slice(h * HEAD, (h + 1) * HEAD)
    return jnp.concatenate([w_key[rows, cols], w_value[rows, cols]], axis=1)


def stacked(parts):
    values = [part[...] for part in parts]
    return values[0] if len(values) == 1 else jnp.concatenate(values, axis=0)


def early_kernel(seq, cut, feature, own, *refs):
    over_x, over_y = refs[: cut + 1], refs[cut + 1 : 2 * cut + 2]
    w_key, w_value, acc = refs[2 * cut + 2 :]
    half, width = over_x[cut].shape
    for h in range(acc.shape[0]):
        pairs = [head_weights(w_key, w_value, feature[j], width, h) for j in range(3)]
        for r, (part_x, part_y) in enumerate(
            ((over_x[:cut], over_y[:1]), (over_x[cut:], over_y[1:]))
        ):
            rows = pl.ds(r * half, half)
            total = jnp.dot(own[seq, rows, :], pairs[0], preferred_element_type=jnp.float32)
            total += jnp.dot(stacked(part_x), pairs[1], preferred_element_type=jnp.float32)
            total += jnp.dot(stacked(part_y), pairs[2], preferred_element_type=jnp.float32)
            acc[h, rows, :] = total


def in_vmem(count):
    return [pl.BlockSpec(memory_space=pltpu.SMEM)] + [pl.BlockSpec(memory_space=pltpu.VMEM)] * count


def early_projection(seq, feature, tokens, over_x, over_y, w_key, w_value):
    seg_len = tokens.shape[1]
    per_head = w_key.shape[1] // HEAD
    cut = len(over_x) - 1
    return pl.pallas_call(
        functools.partial(early_kernel, seq, cut),
        in_specs=in_vmem(2 * cut + 5),
        out_specs=pl.BlockSpec(memory_space=pltpu.VMEM),
        out_shape=jax.ShapeDtypeStruct((per_head, seg_len, 2 * HEAD), jnp.float32),
        compiler_params=pltpu.CompilerParams(vmem_limit_bytes=8 << 20),
        name="early",
    )(feature, tokens, *over_x, *over_y, w_key, w_value)


def late_kernel(heads, groups, before, last, feature, acc, *refs):
    count = sum(len(group) for group in groups)
    far, (w_key, w_value, scale), rest = refs[:count], refs[count : count + 3], refs[count + 3 :]
    width = far[0].shape[1]
    for h in heads:
        pair = head_weights(w_key, w_value, feature[3], width, h)
        total = rest[0][h] if before else None
        used = 0
        for starts in groups:
            pieces = far[used : used + len(starts)]
            used += len(starts)
            spans = [pl.ds(lo, piece.shape[0]) for lo, piece in zip(starts, pieces)]
            base = jnp.concatenate([acc[h, span, :] for span in spans], axis=0)
            now = jnp.concatenate([scale[h, :, span] for span in spans], axis=1)
            kv = base + jnp.dot(stacked(pieces), pair, preferred_element_type=jnp.float32)
            kv = kv.astype(jnp.bfloat16)
            keys_t = kv[:, :HEAD].astype(jnp.float32).T
            high = now.astype(jnp.bfloat16)
            low = (now - high.astype(jnp.float32)).astype(jnp.bfloat16)
            left = jnp.concatenate(
                [
                    (keys_t * now[0:1]).astype(jnp.bfloat16),
                    (keys_t * now[1:2]).astype(jnp.bfloat16),
                    jnp.concatenate([high, low], axis=0),
                ],
                axis=0,
            )
            part = jnp.dot(left, kv, preferred_element_type=jnp.float32)
            total = part if total is None else total + part
        if not last:
            rest[-1][h] = total
            continue
        slabs = []
        for j in range(2):
            norm = total[2 * HEAD + j : 2 * HEAD + j + 1, :HEAD]
            norm = norm + total[2 * HEAD + 8 + j : 2 * HEAD + 8 + j + 1, :HEAD]
            norm = jnp.broadcast_to(norm, (SLAB - HEAD, HEAD))
            slabs.append(jnp.concatenate([total[j * HEAD : (j + 1) * HEAD, HEAD:], norm], axis=0))
        first = feature[4] == 0
        keep, give = rest[-2:]
        keep[h - heads[0]] = jnp.where(first, slabs[0], slabs[1])
        give[h - heads[0]] = jnp.where(first, slabs[1], slabs[0])


def late_memory(heads, groups, before, last, feature, acc, w_key, w_value, scale):
    starts = tuple(tuple(lo for lo, _ in group) for group in groups)
    far = [piece for group in groups for _, piece in group]
    extra = [] if before is None else [before]
    if last:
        shapes = [jax.ShapeDtypeStruct((len(heads), SLAB, HEAD), jnp.float32)] * 2
    else:
        shapes = [jax.ShapeDtypeStruct((len(heads), 2 * HEAD + 16, 2 * HEAD), jnp.float32)]
    return pl.pallas_call(
        functools.partial(late_kernel, heads, starts, bool(extra), last),
        in_specs=in_vmem(4 + len(far) + len(extra)),
        out_specs=[pl.BlockSpec(memory_space=pltpu.VMEM)] * len(shapes),
        out_shape=shapes,
        compiler_params=pltpu.CompilerParams(vmem_limit_bytes=8 << 20),
        name="late",
    )(feature, acc, *far, w_key, w_value, scale, *extra)


def tie(array, *others):
    return lax.optimization_barrier((array,) + others)[0]


def add_over_sp(keep, give):
    halfway = []
    total = keep + swap(give, "sp", 1)
    bit = 2
    while bit < lax.axis_size("sp"):
        wire = lax.optimization_barrier(total.astype(jnp.bfloat16))
        halfway.append(wire)
        total = wire.astype(jnp.float32) + swap(wire, "sp", bit).astype(jnp.float32)
        bit *= 2
    return lax.optimization_barrier(total.astype(jnp.bfloat16)), halfway[-1]


def read_kernel(layout, place, *refs):
    seq_count, _, _ = refs[-4].shape
    slabs, query = refs[:-4], refs[-4]
    matrix_out, norm_out, read_out = refs[-3:]
    per_head = matrix_out.shape[2]
    core = place[0]
    for slab, (b, i, heads) in zip(slabs, layout):
        j = core if i == 0 else 1 - core
        for k, h in enumerate(heads):
            matrix_out[b, j, h] = slab[k, :HEAD, :]
            norm_out[b, j, h : h + 1] = slab[k, HEAD:, :].astype(jnp.float32)[0:1]
    for b in range(seq_count):
        for h in range(per_head):
            q = query[b, :, h * HEAD : (h + 1) * HEAD]
            q_f = q.astype(jnp.float32)
            total = None
            for j in range(2):
                top = jnp.dot(q, matrix_out[b, j, h], preferred_element_type=jnp.float32)
                below = jnp.sum(q_f * norm_out[b, j, h : h + 1], axis=1, keepdims=True)
                part = top / jnp.maximum(jnp.abs(below), 1.0)
                total = part if total is None else total + part
            read_out[b, :, h * HEAD : (h + 1) * HEAD] = total.astype(jnp.bfloat16)


def assemble_and_read(place, layout, slabs, query, per_head):
    seq_count, new_count, width = query.shape
    return pl.pallas_call(
        functools.partial(read_kernel, layout),
        in_specs=[pl.BlockSpec(memory_space=pltpu.SMEM)]
        + [pl.BlockSpec(memory_space=pltpu.VMEM)] * (len(slabs) + 1),
        out_specs=[pl.BlockSpec(memory_space=pltpu.VMEM)] * 3,
        out_shape=[
            jax.ShapeDtypeStruct((seq_count, 2, per_head, HEAD, HEAD), jnp.bfloat16),
            jax.ShapeDtypeStruct((seq_count, 2, per_head, HEAD), jnp.float32),
            jax.ShapeDtypeStruct((seq_count, new_count, width), jnp.bfloat16),
        ],
        compiler_params=pltpu.CompilerParams(vmem_limit_bytes=8 << 20),
        name="read",
    )(place, *slabs, query)


def square_group(tokens, w_key, w_value, w_gate, forget_bias, log_shift, new_query):
    seq_count, seg_len, width = tokens.shape
    per_head = w_key.shape[1] // HEAD
    t = lax.axis_index("tp")
    s = lax.axis_index("sp")
    tp = lax.axis_size("tp")
    core = s % 2
    feature = jnp.stack([t, t ^ 1, t ^ 2, t ^ 3, core]).astype(jnp.int32)
    half = seg_len // 2

    small = half - HEAD if half % HEAD == 0 and half > HEAD else half
    cuts = [[(0, half)]] * (seq_count - 1) + [[(0, small), (small, half)][: 1 + (small < half)]]

    def lead(source, b):
        out = []
        for lo, hi in cuts[b]:
            x_a = swap(source[b, lo:hi], "tp", 1)
            y_b = swap(source[b, half + lo : half + hi], "tp", 2)
            out.append((x_a, y_b))
        return out

    first = lead(tokens, 0)

    gate_rows = lax.dynamic_slice_in_dim(w_gate, t * width, width, 0)
    gate_rows = gate_rows.reshape(width, 4, tp, per_head).transpose(2, 1, 3, 0)
    gate_part = lax.dot_general(
        gate_rows.reshape(tp * 4 * per_head, width),
        tokens.reshape(seq_count * seg_len, width),
        (((1,), (1,)), ((), ())),
        preferred_element_type=jnp.float32,
    ).reshape(tp, 4 * per_head, seq_count * seg_len)
    shares = [
        swap(lax.dynamic_index_in_dim(gate_part, t ^ bit, 0, keepdims=False), "tp", bit)
        for bit in range(1, tp)
    ]
    held = tie(tokens, gate_part)
    over_x, over_y, far = [], [], []
    for b in range(seq_count):
        if b:
            first = lead(held, b)
        x_b = swap(held[b, half:], "tp", 1)
        y_a = swap(held[b, :half], "tp", 2)
        if b == 0:
            shares = lax.optimization_barrier(tuple(shares) + first[0])[: tp - 1]
        far.append([])
        for x_a, y_b in first:
            far[b].append((swap(x_a, "tp", 2), swap(y_b, "tp", 1)))
        over_x.append([pair[0] for pair in first] + [x_b])
        over_y.append([y_a] + [pair[1] for pair in first])
    gates = lax.dynamic_index_in_dim(gate_part, t, 0, keepdims=False)
    for share in shares:
        gates = gates + share
    gates = gates.reshape(4, per_head, seq_count, seg_len).transpose(2, 0, 1, 3)
    bias_own = lax.dynamic_slice_in_dim(forget_bias, t * per_head, per_head, 1)
    weights, totals = decay(gates, bias_own, log_shift)
    tops = jnp.stack([totals, jnp.max(weights, axis=-1)])
    every = lax.all_gather(tops, "sp")
    every_total, every_top = every[:, 0], every[:, 1]
    sources = jnp.arange(every_total.shape[0])
    direction = jnp.arange(2)[None, None, None, :, None]
    later, sooner = sources[None, :] > sources[:, None], sources[None, :] < sources[:, None]
    counted = jnp.where(direction == 0, later[..., None, None, None], sooner[..., None, None, None])
    every_passed = jnp.sum(jnp.where(counted, every_total[None], 0.0), axis=1)
    cache_max = jnp.maximum(jnp.sum(every_total, axis=0), jnp.max(every_top + every_passed, axis=0))
    passed = lax.dynamic_index_in_dim(every_passed, s, 0, keepdims=False)
    scale = jnp.exp(weights + (passed - cache_max)[..., None]) * HEAD ** (-0.5)
    scale = scale.transpose(0, 2, 1, 3)
    scale = jnp.concatenate([scale, jnp.zeros((seq_count, per_head, 6, seg_len), jnp.float32)], axis=2)

    slabs, layout = [], []
    for b in range(seq_count):
        seen_x, seen_y = over_x[b], over_y[b]
        if slabs:
            seen_x = [tie(part, halfway) for part in seen_x]
            seen_y = [tie(part, halfway) for part in seen_y]
        acc = early_projection(b, feature, tokens, seen_x, seen_y, w_key, w_value)
        shared = (feature, acc, w_key, w_value, scale[b])
        before = None
        *sooner, (far_a, far_b) = far[b]
        every = tuple(range(per_head))
        for (lo, _), (part_a, part_b) in zip(cuts[b], sooner):
            part_a, part_b = tie(part_a, *slabs), tie(part_b, *slabs)
            groups = [[(lo, part_a)], [(half + lo, part_b)]]
            (before,) = late_memory(every, groups, before, False, *shared)
        lo = cuts[b][-1][0]
        ahead = slabs if before is None else slabs + [before]
        if ahead:
            far_a, far_b = tie(far_a, *ahead), tie(far_b, *ahead)
        groups = [[(lo, far_a)], [(half + lo, far_b)]]
        if sooner:
            groups = [groups[0] + groups[1]]
        parts = 2 if b == seq_count - 1 else 1
        own = []
        for k in range(parts):
            heads = every[per_head * k // parts : per_head * (k + 1) // parts]
            keep, give = late_memory(heads, groups, before, True, *shared)
            mine, halfway = add_over_sp(keep, give)
            own += [mine, swap(mine, "sp", 1)]
            layout += [(b, 0, heads), (b, 1, heads)]
        slabs += own

    place = core.astype(jnp.int32)[None]
    cache_matrix, norm, first_read = assemble_and_read(place, layout, slabs, new_query, per_head)
    return (cache_matrix, norm, cache_max, first_read)


def solution(mesh):
    def on_device(tokens, w_key, *rest):
        square = mesh.shape["tp"] == 4 and mesh.shape["sp"] == 2 * (w_key.shape[1] // HEAD)
        return (square_group if square else any_mesh)(tokens, w_key, *rest)

    return jax.shard_map(
        on_device,
        mesh=mesh,
        in_specs=(
            P(None, "sp", "tp"),
            P(None, "tp"),
            P(None, "tp"),
            P(),
            P(),
            P(None, None, "tp", "sp"),
            P(None, "sp", "tp"),
        ),
        out_specs=(
            P(None, None, "tp", None, None),
            P(None, None, "tp", None),
            P(None, None, "tp"),
            P(None, "sp", "tp"),
        ),
        check_vma=False,
    )
```

profile of v0, /device:TPU:0, one launch (start us, length us, event | category | flops | bytes accessed | tf_op | source)
XLA Modules:
  0.0 159.6 jit_solution(2352979762192174617)
XLA Ops:
  0.7 1.0 copy-done
  2.0 3.1 %fusion.21 = f32[4,16,1536]{2,1,0:T(8,128)S(1)} fusion(bf16[4,16,1024]{2,1,0:T(8,128)(2,1)S(1)} %dot_general.5, bf16[1536,1024,1]{1,0,2:T(8,128)(2,1)} %bitcast.68), kind=kOutput, calls=%fused_computation.73 | convolution fusion | flops 201326592 | bytes 3670016 | tf_op jit(solution)/shard_map/dot_general | solution.py:296
  5.1 0.7 dynamic-slice_bitcast_fusion
  5.8 3.0 %collective-permute-start.6 = (f32[16,1536]{1,0:T(8,128)S(1)}, f32[16,1536]{1,0:T(8,128)S(1)}, u32[]{:S(2)}, u32[]{:S(2)}) collective-permute-start(f32[16,1536]{1,0:T(8,128)S(1)} %get-tuple-element.66), channel_id=1, source_target_pairs={{0,1},{1,0},{2,3},{3,2},{4,5},{5,4},{6,7},{7,6},{8,9},{9,8},{10,11... | collective-permute-start | bytes 294920 | tf_op jit(solution)/shard_map/ppermute | solution.py:104
  8.7 1.5 collective-permute-start.7
  10.3 1.3 slice_bitcast_fusion.2
  11.6 2.0 %collective-permute-start = (bf16[384,1024]{1,0:T(8,128)(2,1)}, bf16[384,1024]{1,0:T(8,128)(2,1)S(1)}, u32[]{:S(2)}, u32[]{:S(2)}) collective-permute-start(bf16[384,1024]{1,0:T(8,128)(2,1)} %get-tuple-element.63), channel_id=1, source_target_pairs={{0,1},{1,0},{2,3},{3,2},{4,5},{5,4},{6,7},{7,6},{8,9},{9,8},{10,11... | collective-permute-start | bytes 2359304 | tf_op jit(solution)/shard_map/ppermute | solution.py:104
  13.5 1.5 collective-permute-start.3
  15.2 0.6 fusion.18
  15.8 3.5 %slice_bitcast_fusion = (bf16[384,1024]{1,0:T(8,128)(2,1)}, bf16[384,1024]{1,0:T(8,128)(2,1)}, bf16[384,1024]{1,0:T(8,128)(2,1)}, bf16[384,1024]{1,0:T(8,128)(2,1)}) fusion(bf16[2,768,1024]{2,1,0:T(8,128)(2,1)} %own.3), kind=kLoop, calls=%fused_computation | loop fusion | bytes 6291456 | tf_op jit(solution)/shard_map/squeeze | solution.py:312
  19.4 0.6 slice_bitcast_fusion.11
  20.0 0.5 collective-permute-start.1
  20.6 12.1 %collective-permute-done.refs_0_ = bf16[384,1024]{1,0:T(8,128)(2,1)S(1)} collective-permute-done((bf16[384,1024]{1,0:T(8,128)(2,1)}, bf16[384,1024]{1,0:T(8,128)(2,1)S(1)}, u32[]{:S(2)}, u32[]{:S(2)}) %collective-permute-start) | collective-permute-done | bytes 786464 | tf_op jit(solution)/shard_map/ppermute | solution.py:104
  32.7 1.4 collective-permute-done.3.refs_3_
  34.1 1.0 fusion.3
  35.2 1.2 fusion.16
  36.5 4.5 %reduce-window.6 = f32[2,2,4,6,128]{4,3,2,1,0:T(8,128)S(1)} reduce-window(f32[2,2,4,6,128]{4,3,2,1,0:T(8,128)S(1)} %copy.72, f32[]{:T(128)} %constant.60.clone.1), window={size=1x1x1x1x128 pad=0_0x0_0x0_0x0_0x127_0}, to_apply=%region_0.1 | reduce-window | flops 1560576 | bytes 98308 | tf_op jit(solution)/shard_map/reduce-window
  41.0 0.2 slice_reduce_fusion
  41.2 0.7 reduce-window.9
  42.1 0.2 slice_reduce_fusion.1
  42.4 0.1 fusion.13
  42.6 14.5 %all-gather = f32[16,2,2,4]{3,2,1,0:T(2,128)S(1)} all-gather(f32[2,2,2,4]{3,2,1,0:T(2,128)S(1)} %pad_maximum_fusion.2), channel_id=2, replica_groups=mesh['sp'=8,'tp'=4] {'sp'}, dimensions={0}, use_global_device_ids=true | all-gather | bytes 1152 | tf_op jit(solution)/shard_map/all_gather | solution.py:327
  57.3 1.5 collective-permute-start.4
  58.8 0.5 collective-permute-start.5
  59.5 0.2 dynamic-slice_reduce_fusion
  59.7 0.6 fusion.15
  60.4 2.2 %copy-done.1 = bf16[4096,512]{1,0:T(8,128)(2,1)S(1)} copy-done((bf16[4096,512]{1,0:T(8,128)(2,1)S(1)}, bf16[4096,512]{1,0:T(8,128)(2,1)}, u32[]{:S(2)}) %copy-start.1) | copy-done | bytes 4194328
  62.6 2.2 %copy-done.3 = bf16[4096,512]{1,0:T(8,128)(2,1)S(1)} copy-done((bf16[4096,512]{1,0:T(8,128)(2,1)S(1)}, bf16[4096,512]{1,0:T(8,128)(2,1)}, u32[]{:S(2)}) %copy-start.3) | copy-done | bytes 4194328
  64.8 1.9 %copy-done.6 = bf16[2,768,1024]{2,1,0:T(8,128)(2,1)S(1)} copy-done((bf16[2,768,1024]{2,1,0:T(8,128)(2,1)S(1)}, bf16[2,768,1024]{2,1,0:T(8,128)(2,1)}, u32[]{:S(2)}) %copy-start.6) | copy-done | bytes 3145752
  66.7 6.4 %early.2.acc = f32[4,768,256]{2,1,0:T(8,128)S(1)} custom-call(s32[5]{0:T(128)S(1)} %stack.40.feature, bf16[2,768,1024]{2,1,0:T(8,128)(2,1)S(1)} %copy-done.6, bf16[384,1024]{1,0:T(8,128)(2,1)S(1)} %collective-permute-done.refs_0_, bf16[384,1024]{1,0:T(8,128)(2,1)S(1)} %collective-permute-done.1.refs_1_, bf16[384,1024]{1,0:T(8,128)(2,1)} %collective-permute-done.2.refs_2_, ...), custom_call_target="tpu_custom_call" | custom-call | tf_op jit(solution)/shard_map/early/pallas_call | solution.py:142
  73.2 4.0 %collective-permute-done.4.refs_0_ = bf16[384,1024]{1,0:T(8,128)(2,1)} collective-permute-done((bf16[384,1024]{1,0:T(8,128)(2,1)S(1)}, bf16[384,1024]{1,0:T(8,128)(2,1)}, u32[]{:S(2)}, u32[]{:S(2)}) %collective-permute-start.4) | collective-permute-done | bytes 786464 | tf_op jit(solution)/shard_map/ppermute | solution.py:104
  77.2 1.2 collective-permute-done.5.refs_1_
  78.5 5.0 %late.4 = (f32[4,136,128]{2,1,0:T(8,128)S(1)}, f32[4,136,128]{2,1,0:T(8,128)S(1)}) custom-call(s32[5]{0:T(128)S(1)} %stack.40.feature, f32[4,768,256]{2,1,0:T(8,128)S(1)} %early.2.acc, bf16[384,1024]{1,0:T(8,128)(2,1)} %collective-permute-done.4.refs_0_, bf16[384,1024]{1,0:T(8,128)(2,1)} %collective-permute-done.5.refs_1_, bf16[4096,512]{1,0:T(8,128)(2,1)S(1)} %copy-done.2, ...), custom_call_target="tpu_custom_call" | custom-call | tf_op jit(solution)/shard_map/late/pallas_call | solution.py:204
  83.6 0.6 collective-permute-start.17
  84.2 0.5 collective-permute-start.13
  84.8 1.5 collective-permute-start.16
  86.3 1.6 collective-permute-start.14
  87.9 0.5 collective-permute-start.15
  88.4 16.2 %collective-permute-done.14.refs_1_ = bf16[128,1024]{1,0:T(8,128)(2,1)S(1)} collective-permute-done((bf16[128,1024]{1,0:T(8,128)(2,1)S(1)}, bf16[128,1024]{1,0:T(8,128)(2,1)S(1)}, u32[]{:S(2)}, u32[]{:S(2)}) %collective-permute-start.14) | collective-permute-done | bytes 262176 | tf_op jit(solution)/shard_map/ppermute | solution.py:104
  104.6 1.6 collective-permute-start.10
  106.2 1.5 collective-permute-start.18
  107.7 0.5 collective-permute-start.21
  108.2 1.4 collective-permute-done.10
  109.7 1.5 collective-permute-start.20
  111.3 9.7 %collective-permute-done.18.refs_5_ = bf16[128,1024]{1,0:T(8,128)(2,1)S(1)} collective-permute-done((bf16[128,1024]{1,0:T(8,128)(2,1)S(1)}, bf16[128,1024]{1,0:T(8,128)(2,1)S(1)}, u32[]{:S(2)}, u32[]{:S(2)}) %collective-permute-start.18) | collective-permute-done | bytes 262176 | tf_op jit(solution)/shard_map/ppermute | solution.py:104
  121.0 0.6 collective-permute-start.11
  121.5 0.5 collective-permute-start.22
  122.1 7.5 %collective-permute-done.11 = bf16[4,136,128]{2,1,0:T(8,128)(2,1)S(1)} collective-permute-done((bf16[4,136,128]{2,1,0:T(8,128)(2,1)S(1)}, bf16[4,136,128]{2,1,0:T(8,128)(2,1)S(1)}, u32[]{:S(2)}, u32[]{:S(2)}) %collective-permute-start.11) | collective-permute-done | bytes 139296 | tf_op jit(solution)/shard_map/ppermute | solution.py:104
  129.6 0.5 collective-permute-start.19
  130.2 5.6 %early.3.acc = f32[4,768,256]{2,1,0:T(8,128)S(1)} custom-call(s32[5]{0:T(128)S(1)} %stack.40.feature, bf16[2,768,1024]{2,1,0:T(8,128)(2,1)S(1)} %copy-done.6, bf16[256,1024]{1,0:T(8,128)(2,1)S(1)} %collective-permute-done.13.refs_0_, bf16[128,1024]{1,0:T(8,128)(2,1)S(1)} %collective-permute-done.14.refs_1_, ...), custom_call_target="tpu_custom_call" | custom-call | tf_op jit(solution)/shard_map/early/pallas_call | solution.py:142
  135.9 3.3 %late.5.refs_5_ = f32[4,272,256]{2,1,0:T(8,128)S(1)} custom-call(s32[5]{0:T(128)S(1)} %stack.40.feature, f32[4,768,256]{2,1,0:T(8,128)S(1)} %early.3.acc, bf16[256,1024]{1,0:T(8,128)(2,1)S(1)} %collective-permute-done.20.refs_0_, bf16[256,1024]{1,0:T(8,128)(2,1)S(1)} %collective-permute-done.21.refs_1_, bf16[4096,512]{1,0:T(8,128)(2,1)S(1)} %copy-done.2, ...), custom_call_target="tpu_custom_call" | custom-call | tf_op jit(solution)/shard_map/late/pallas_call | solution.py:204
  139.2 1.7 %late.7 = (f32[2,136,128]{2,1,0:T(8,128)S(1)}, f32[2,136,128]{2,1,0:T(8,128)S(1)}) custom-call(s32[5]{0:T(128)S(1)} %stack.40.feature, f32[4,768,256]{2,1,0:T(8,128)S(1)} %early.3.acc, bf16[128,1024]{1,0:T(8,128)(2,1)S(1)} %collective-permute-done.19.refs_0_, bf16[128,1024]{1,0:T(8,128)(2,1)S(1)} %collective-permute-done.22.refs_1_, ...), custom_call_target="tpu_custom_call" | custom-call | tf_op jit(solution)/shard_map/late/pallas_call | solution.py:204
  140.9 0.6 collective-permute-start.27
  141.5 1.7 %late.6 = (f32[2,136,128]{2,1,0:T(8,128)S(1)}, f32[2,136,128]{2,1,0:T(8,128)S(1)}) custom-call(s32[5]{0:T(128)S(1)} %stack.40.feature, f32[4,768,256]{2,1,0:T(8,128)S(1)} %early.3.acc, bf16[128,1024]{1,0:T(8,128)(2,1)S(1)} %collective-permute-done.19.refs_0_, bf16[128,1024]{1,0:T(8,128)(2,1)S(1)} %collective-permute-done.22.refs_1_, ...), custom_call_target="tpu_custom_call" | custom-call | tf_op jit(solution)/shard_map/late/pallas_call | solution.py:204
  143.4 1.2 collective-permute-done.23
  144.6 0.9 collective-permute-start.24
  145.5 2.9 %collective-permute-done.28 = bf16[2,136,128]{2,1,0:T(8,128)(2,1)S(1)} collective-permute-done((bf16[2,136,128]{2,1,0:T(8,128)(2,1)S(1)}, bf16[2,136,128]{2,1,0:T(8,128)(2,1)S(1)}, u32[]{:S(2)}, u32[]{:S(2)}) %collective-permute-start.28) | collective-permute-done | bytes 69664 | tf_op jit(solution)/shard_map/ppermute | solution.py:104
  148.5 0.2 collective-permute-start.29
  148.7 0.8 collective-permute-done.24
  149.5 2.1 %collective-permute-start.25 = (bf16[2,136,128]{2,1,0:T(8,128)(2,1)S(1)}, bf16[2,136,128]{2,1,0:T(8,128)(2,1)S(1)}, u32[]{:S(2)}, u32[]{:S(2)}) collective-permute-start(bf16[2,136,128]{2,1,0:T(8,128)(2,1)S(1)} %add_convert_fusion.7), channel_id=1, source_target_pairs={{0,16},{4,20},{8,24},{12,28},{16,0},{20,4},{24,8},{28,12},{1,17},{... | collective-permute-start | bytes 208904 | tf_op jit(solution)/shard_map/ppermute | solution.py:104
  151.5 4.4 %collective-permute-done.29 = bf16[2,136,128]{2,1,0:T(8,128)(2,1)S(1)} collective-permute-done((bf16[2,136,128]{2,1,0:T(8,128)(2,1)S(1)}, bf16[2,136,128]{2,1,0:T(8,128)(2,1)S(1)}, u32[]{:S(2)}, u32[]{:S(2)}) %collective-permute-start.29) | collective-permute-done | bytes 69664 | tf_op jit(solution)/shard_map/ppermute | solution.py:104
  156.1 1.1 collective-permute-done.25
  157.3 1.2 collective-permute-done.26.refs_3_
  158.5 1.2 read.1
  (86 shorter events, 2.6 us)
Async XLA Ops:
  0.6 1.0 copy-start
  1.9 8.3 %copy-start.5 = (bf16[2,768,1024]{2,1,0:T(8,128)(2,1)S(1)}, bf16[2,768,1024]{2,1,0:T(8,128)(2,1)}, u32[]{:S(2)}) copy-start(bf16[2,768,1024]{2,1,0:T(8,128)(2,1)} %own.3) | copy-start | bytes 9437188
  1.9 13.2 %copy-start.11 = (f32[2,16]{1,0:T(2,128)S(1)}, f32[2,16]{1,0:T(2,128)}, u32[]{:S(2)}) copy-start(f32[2,16]{1,0:T(2,128)} %param.11) | copy-start | bytes 388
  2.0 13.2 %copy-start.10 = (f32[2,4,4,768]{3,2,1,0:T(4,128)S(1)}, f32[2,4,4,768]{3,2,1,0:T(4,128)}, u32[]{:S(2)}) copy-start(f32[2,4,4,768]{3,2,1,0:T(4,128)} %param.12) | copy-start | bytes 294916
  5.8 14.3 %collective-permute-start.6 = (f32[16,1536]{1,0:T(8,128)S(1)}, f32[16,1536]{1,0:T(8,128)S(1)}, u32[]{:S(2)}, u32[]{:S(2)}) collective-permute-start(f32[16,1536]{1,0:T(8,128)S(1)} %get-tuple-element.66), channel_id=1, source_target_pairs={{0,1},{1,0},{2,3},{3,2},{4,5},{5,4},{6,7},{7,6},{8,9},{9,8},{10,11... | collective-permute-start | bytes 294920 | tf_op jit(solution)/shard_map/ppermute | solution.py:104
  8.7 11.8 %collective-permute-start.7 = (f32[16,1536]{1,0:T(8,128)}, f32[16,1536]{1,0:T(8,128)}, u32[]{:S(2)}, u32[]{:S(2)}) collective-permute-start(f32[16,1536]{1,0:T(8,128)} %get-tuple-element.65), channel_id=1, source_target_pairs={{0,2},{1,3},{2,0},{3,1},{4,6},{5,7},{6,4},{7,5},{8,10},{9,11},{10,... | collective-permute-start | bytes 294920 | tf_op jit(solution)/shard_map/ppermute | solution.py:104
  10.2 10.4 %collective-permute-start.8 = (f32[16,1536]{1,0:T(8,128)S(1)}, f32[16,1536]{1,0:T(8,128)}, u32[]{:S(2)}, u32[]{:S(2)}) collective-permute-start(f32[16,1536]{1,0:T(8,128)S(1)} %get-tuple-element.64), channel_id=1, source_target_pairs={{0,3},{1,2},{2,1},{3,0},{4,7},{5,6},{6,5},{7,4},{8,11},{9,10},{10,... | collective-permute-start | bytes 294920 | tf_op jit(solution)/shard_map/ppermute | solution.py:104
  11.6 21.2 %collective-permute-start = (bf16[384,1024]{1,0:T(8,128)(2,1)}, bf16[384,1024]{1,0:T(8,128)(2,1)S(1)}, u32[]{:S(2)}, u32[]{:S(2)}) collective-permute-start(bf16[384,1024]{1,0:T(8,128)(2,1)} %get-tuple-element.63), channel_id=1, source_target_pairs={{0,1},{1,0},{2,3},{3,2},{4,5},{5,4},{6,7},{7,6},{8,9},{9,8},{10,11... | collective-permute-start | bytes 2359304 | tf_op jit(solution)/shard_map/ppermute | solution.py:104
  13.5 20.6 %collective-permute-start.3 = (bf16[384,1024]{1,0:T(8,128)(2,1)}, bf16[384,1024]{1,0:T(8,128)(2,1)S(1)}, u32[]{:S(2)}, u32[]{:S(2)}) collective-permute-start(bf16[384,1024]{1,0:T(8,128)(2,1)} %get-tuple-element.62), channel_id=1, source_target_pairs={{0,2},{1,3},{2,0},{3,1},{4,6},{5,7},{6,4},{7,5},{8,10},{9,11},{10,... | collective-permute-start | bytes 2359304 | tf_op jit(solution)/shard_map/ppermute | solution.py:104
  20.0 40.4 %collective-permute-start.1 = (bf16[384,1024]{1,0:T(8,128)(2,1)}, bf16[384,1024]{1,0:T(8,128)(2,1)S(1)}, u32[]{:S(2)}, u32[]{:S(2)}) collective-permute-start(bf16[384,1024]{1,0:T(8,128)(2,1)} %get-tuple-element.61), channel_id=1, source_target_pairs={{0,1},{1,0},{2,3},{3,2},{4,5},{5,4},{6,7},{7,6},{8,9},{9,8},{10,11... | collective-permute-start | bytes 2359304 | tf_op jit(solution)/shard_map/ppermute | solution.py:104
  20.6 39.9 %collective-permute-start.2 = (bf16[384,1024]{1,0:T(8,128)(2,1)}, bf16[384,1024]{1,0:T(8,128)(2,1)}, u32[]{:S(2)}, u32[]{:S(2)}) collective-permute-start(bf16[384,1024]{1,0:T(8,128)(2,1)} %get-tuple-element.60), channel_id=1, source_target_pairs={{0,2},{1,3},{2,0},{3,1},{4,6},{5,7},{6,4},{7,5},{8,10},{9,11},{10,... | collective-permute-start | bytes 2359304 | tf_op jit(solution)/shard_map/ppermute | solution.py:104
  57.3 19.9 %collective-permute-start.4 = (bf16[384,1024]{1,0:T(8,128)(2,1)S(1)}, bf16[384,1024]{1,0:T(8,128)(2,1)}, u32[]{:S(2)}, u32[]{:S(2)}) collective-permute-start(bf16[384,1024]{1,0:T(8,128)(2,1)S(1)} %collective-permute-done.refs_0_), channel_id=1, source_target_pairs={{0,2},{1,3},{2,0},{3,1},{4,6},{5,7},{6,4},{7,5},{8,10},{9,11},{10,... | collective-permute-start | bytes 2359304 | tf_op jit(solution)/shard_map/ppermute | solution.py:104
  58.8 19.6 %collective-permute-start.5 = (bf16[384,1024]{1,0:T(8,128)(2,1)S(1)}, bf16[384,1024]{1,0:T(8,128)(2,1)}, u32[]{:S(2)}, u32[]{:S(2)}) collective-permute-start(bf16[384,1024]{1,0:T(8,128)(2,1)S(1)} %collective-permute-done.3.refs_3_), channel_id=1, source_target_pairs={{0,1},{1,0},{2,3},{3,2},{4,5},{5,4},{6,7},{7,6},{8,9},{9,8},{10,11... | collective-permute-start | bytes 2359304 | tf_op jit(solution)/shard_map/ppermute | solution.py:104
  60.4 2.2 %copy-start.1 = (bf16[4096,512]{1,0:T(8,128)(2,1)S(1)}, bf16[4096,512]{1,0:T(8,128)(2,1)}, u32[]{:S(2)}) copy-start(bf16[4096,512]{1,0:T(8,128)(2,1)} %refs_2_.7) | copy-start | bytes 12582916
  62.6 2.2 %copy-start.3 = (bf16[4096,512]{1,0:T(8,128)(2,1)S(1)}, bf16[4096,512]{1,0:T(8,128)(2,1)}, u32[]{:S(2)}) copy-start(bf16[4096,512]{1,0:T(8,128)(2,1)} %refs_3_.7) | copy-start | bytes 12582916
  64.8 1.9 %copy-start.6 = (bf16[2,768,1024]{2,1,0:T(8,128)(2,1)S(1)}, bf16[2,768,1024]{2,1,0:T(8,128)(2,1)}, u32[]{:S(2)}) copy-start(bf16[2,768,1024]{2,1,0:T(8,128)(2,1)} %own.3) | copy-start | bytes 9437188
  66.7 11.8 %copy-start.2 = (bf16[4096,512]{1,0:T(8,128)(2,1)S(1)}, bf16[4096,512]{1,0:T(8,128)(2,1)}, u32[]{:S(2)}) copy-start(bf16[4096,512]{1,0:T(8,128)(2,1)} %refs_2_.7) | copy-start | bytes 12582916
  66.7 11.8 %copy-start.4 = (bf16[4096,512]{1,0:T(8,128)(2,1)S(1)}, bf16[4096,512]{1,0:T(8,128)(2,1)}, u32[]{:S(2)}) copy-start(bf16[4096,512]{1,0:T(8,128)(2,1)} %refs_3_.7) | copy-start | bytes 12582916
  78.5 6.3 %copy-start.9 = (bf16[384,1024]{1,0:T(8,128)(2,1)S(1)}, bf16[384,1024]{1,0:T(8,128)(2,1)}, u32[]{:S(2)}) copy-start(bf16[384,1024]{1,0:T(8,128)(2,1)} %get-tuple-element.58) | copy-start | bytes 2359300
  83.5 4.4 %copy-start.8 = (bf16[384,1024]{1,0:T(8,128)(2,1)S(1)}, bf16[384,1024]{1,0:T(8,128)(2,1)}, u32[]{:S(2)}) copy-start(bf16[384,1024]{1,0:T(8,128)(2,1)} %get-tuple-element.59) | copy-start | bytes 2359300
  83.5 4.4 %collective-permute-start.9 = (f32[4,136,128]{2,1,0:T(8,128)S(1)}, f32[4,136,128]{2,1,0:T(8,128)S(1)}, u32[]{:S(2)}, u32[]{:S(2)}) collective-permute-start(f32[4,136,128]{2,1,0:T(8,128)S(1)} %get-tuple-element.32), channel_id=1, source_target_pairs={{0,4},{4,0},{8,12},{12,8},{16,20},{20,16},{24,28},{28,24},{1,5},{5... | collective-permute-start | bytes 835592 | tf_op jit(solution)/shard_map/ppermute | solution.py:104
  83.6 22.5 %collective-permute-start.17 = (bf16[256,1024]{1,0:T(8,128)(2,1)S(1)}, bf16[256,1024]{1,0:T(8,128)(2,1)S(1)}, u32[]{:S(2)}, u32[]{:S(2)}) collective-permute-start(bf16[256,1024]{1,0:T(8,128)(2,1)S(1)} %get-tuple-element.56), channel_id=1, source_target_pairs={{0,2},{1,3},{2,0},{3,1},{4,6},{5,7},{6,4},{7,5},{8,10},{9,11},{10,... | collective-permute-start | bytes 1572872 | tf_op jit(solution)/shard_map/ppermute | solution.py:104
  84.2 23.5 %collective-permute-start.13 = (bf16[256,1024]{1,0:T(8,128)(2,1)S(1)}, bf16[256,1024]{1,0:T(8,128)(2,1)S(1)}, u32[]{:S(2)}, u32[]{:S(2)}) collective-permute-start(bf16[256,1024]{1,0:T(8,128)(2,1)S(1)} %get-tuple-element.57), channel_id=1, source_target_pairs={{0,1},{1,0},{2,3},{3,2},{4,5},{5,4},{6,7},{7,6},{8,9},{9,8},{10,11... | collective-permute-start | bytes 1572872 | tf_op jit(solution)/shard_map/ppermute | solution.py:104
  84.8 36.8 %collective-permute-start.16 = (bf16[384,1024]{1,0:T(8,128)(2,1)S(1)}, bf16[384,1024]{1,0:T(8,128)(2,1)S(1)}, u32[]{:S(2)}, u32[]{:S(2)}) collective-permute-start(bf16[384,1024]{1,0:T(8,128)(2,1)S(1)} %copy-done.9), channel_id=1, source_target_pairs={{0,2},{1,3},{2,0},{3,1},{4,6},{5,7},{6,4},{7,5},{8,10},{9,11},{10,... | collective-permute-start | bytes 2359304 | tf_op jit(solution)/shard_map/ppermute | solution.py:104
  86.3 18.3 %collective-permute-start.14 = (bf16[128,1024]{1,0:T(8,128)(2,1)S(1)}, bf16[128,1024]{1,0:T(8,128)(2,1)S(1)}, u32[]{:S(2)}, u32[]{:S(2)}) collective-permute-start(bf16[128,1024]{1,0:T(8,128)(2,1)S(1)} %get-tuple-element.55), channel_id=1, source_target_pairs={{0,1},{1,0},{2,3},{3,2},{4,5},{5,4},{6,7},{7,6},{8,9},{9,8},{10,11... | collective-permute-start | bytes 786440 | tf_op jit(solution)/shard_map/ppermute | solution.py:104
  87.9 42.3 %collective-permute-start.15 = (bf16[384,1024]{1,0:T(8,128)(2,1)S(1)}, bf16[384,1024]{1,0:T(8,128)(2,1)S(1)}, u32[]{:S(2)}, u32[]{:S(2)}) collective-permute-start(bf16[384,1024]{1,0:T(8,128)(2,1)S(1)} %copy-done.8), channel_id=1, source_target_pairs={{0,1},{1,0},{2,3},{3,2},{4,5},{5,4},{6,7},{7,6},{8,9},{9,8},{10,11... | collective-permute-start | bytes 2359304 | tf_op jit(solution)/shard_map/ppermute | solution.py:104
  104.6 5.1 %collective-permute-start.10 = (bf16[4,136,128]{2,1,0:T(8,128)(2,1)S(1)}, bf16[4,136,128]{2,1,0:T(8,128)(2,1)S(1)}, u32[]{:S(2)}, u32[]{:S(2)}) collective-permute-start(bf16[4,136,128]{2,1,0:T(8,128)(2,1)S(1)} %add_convert_fusion.2), channel_id=1, source_target_pairs={{0,8},{4,12},{8,0},{12,4},{16,24},{20,28},{24,16},{28,20},{1,9},{5... | collective-permute-start | bytes 417800 | tf_op jit(solution)/shard_map/ppermute | solution.py:104
  106.2 14.8 %collective-permute-start.18 = (bf16[128,1024]{1,0:T(8,128)(2,1)S(1)}, bf16[128,1024]{1,0:T(8,128)(2,1)S(1)}, u32[]{:S(2)}, u32[]{:S(2)}) collective-permute-start(bf16[128,1024]{1,0:T(8,128)(2,1)S(1)} %get-tuple-element.54), channel_id=1, source_target_pairs={{0,2},{1,3},{2,0},{3,1},{4,6},{5,7},{6,4},{7,5},{8,10},{9,11},{10,... | collective-permute-start | bytes 786440 | tf_op jit(solution)/shard_map/ppermute | solution.py:104
  107.7 28.1 %collective-permute-start.21 = (bf16[256,1024]{1,0:T(8,128)(2,1)S(1)}, bf16[256,1024]{1,0:T(8,128)(2,1)S(1)}, u32[]{:S(2)}, u32[]{:S(2)}) collective-permute-start(bf16[256,1024]{1,0:T(8,128)(2,1)S(1)} %collective-permute-done.17.refs_4_), channel_id=1, source_target_pairs={{0,1},{1,0},{2,3},{3,2},{4,5},{5,4},{6,7},{7,6},{8,9},{9,8},{10,11... | collective-permute-start | bytes 1572872 | tf_op jit(solution)/shard_map/ppermute | solution.py:104
  109.7 26.2 %collective-permute-start.20 = (bf16[256,1024]{1,0:T(8,128)(2,1)S(1)}, bf16[256,1024]{1,0:T(8,128)(2,1)S(1)}, u32[]{:S(2)}, u32[]{:S(2)}) collective-permute-start(bf16[256,1024]{1,0:T(8,128)(2,1)S(1)} %collective-permute-done.13.refs_0_), channel_id=1, source_target_pairs={{0,2},{1,3},{2,0},{3,1},{4,6},{5,7},{6,4},{7,5},{8,10},{9,11},{10,... | collective-permute-start | bytes 1572872 | tf_op jit(solution)/shard_map/ppermute | solution.py:104
  121.0 8.6 %collective-permute-start.11 = (bf16[4,136,128]{2,1,0:T(8,128)(2,1)S(1)}, bf16[4,136,128]{2,1,0:T(8,128)(2,1)S(1)}, u32[]{:S(2)}, u32[]{:S(2)}) collective-permute-start(bf16[4,136,128]{2,1,0:T(8,128)(2,1)S(1)} %add_convert_fusion.1), channel_id=1, source_target_pairs={{0,16},{4,20},{8,24},{12,28},{16,0},{20,4},{24,8},{28,12},{1,17},{... | collective-permute-start | bytes 417800 | tf_op jit(solution)/shard_map/ppermute | solution.py:104
  121.5 17.6 %collective-permute-start.22 = (bf16[128,1024]{1,0:T(8,128)(2,1)S(1)}, bf16[128,1024]{1,0:T(8,128)(2,1)S(1)}, u32[]{:S(2)}, u32[]{:S(2)}) collective-permute-start(bf16[128,1024]{1,0:T(8,128)(2,1)S(1)} %collective-permute-done.18.refs_5_), channel_id=1, source_target_pairs={{0,1},{1,0},{2,3},{3,2},{4,5},{5,4},{6,7},{7,6},{8,9},{9,8},{10,11... | collective-permute-start | bytes 786440 | tf_op jit(solution)/shard_map/ppermute | solution.py:104
  129.6 9.6 %collective-permute-start.19 = (bf16[128,1024]{1,0:T(8,128)(2,1)S(1)}, bf16[128,1024]{1,0:T(8,128)(2,1)S(1)}, u32[]{:S(2)}, u32[]{:S(2)}) collective-permute-start(bf16[128,1024]{1,0:T(8,128)(2,1)S(1)} %collective-permute-done.14.refs_1_), channel_id=1, source_target_pairs={{0,2},{1,3},{2,0},{3,1},{4,6},{5,7},{6,4},{7,5},{8,10},{9,11},{10,... | collective-permute-start | bytes 786440 | tf_op jit(solution)/shard_map/ppermute | solution.py:104
  130.2 5.7 %collective-permute-start.12 = (bf16[4,136,128]{2,1,0:T(8,128)(2,1)S(1)}, bf16[4,136,128]{2,1,0:T(8,128)(2,1)S(1)}, u32[]{:S(2)}, u32[]{:S(2)}) collective-permute-start(bf16[4,136,128]{2,1,0:T(8,128)(2,1)S(1)} %add_convert_fusion.refs_0_), channel_id=1, source_target_pairs={{0,4},{4,0},{8,12},{12,8},{16,20},{20,16},{24,28},{28,24},{1,5},{5... | collective-permute-start | bytes 417800 | tf_op jit(solution)/shard_map/ppermute | solution.py:104
  140.9 17.6 %copy-start.7 = (bf16[2,128,512]{2,1,0:T(8,128)(2,1)S(1)}, bf16[2,128,512]{2,1,0:T(8,128)(2,1)}, u32[]{:S(2)}) copy-start(bf16[2,128,512]{2,1,0:T(8,128)(2,1)} %refs_6_.3) | copy-start | bytes 786436
  140.9 2.4 %collective-permute-start.27 = (f32[2,136,128]{2,1,0:T(8,128)S(1)}, f32[2,136,128]{2,1,0:T(8,128)S(1)}, u32[]{:S(2)}, u32[]{:S(2)}) collective-permute-start(f32[2,136,128]{2,1,0:T(8,128)S(1)} %get-tuple-element.46), channel_id=1, source_target_pairs={{0,4},{4,0},{8,12},{12,8},{16,20},{20,16},{24,28},{28,24},{1,5},{5... | collective-permute-start | bytes 417800 | tf_op jit(solution)/shard_map/ppermute | solution.py:104
  143.2 1.4 collective-permute-start.23
  143.3 5.1 %collective-permute-start.28 = (bf16[2,136,128]{2,1,0:T(8,128)(2,1)S(1)}, bf16[2,136,128]{2,1,0:T(8,128)(2,1)S(1)}, u32[]{:S(2)}, u32[]{:S(2)}) collective-permute-start(bf16[2,136,128]{2,1,0:T(8,128)(2,1)S(1)} %add_convert_fusion.5), channel_id=1, source_target_pairs={{0,8},{4,12},{8,0},{12,4},{16,24},{20,28},{24,16},{28,20},{1,9},{5... | collective-permute-start | bytes 208904 | tf_op jit(solution)/shard_map/ppermute | solution.py:104
  144.6 4.8 %collective-permute-start.24 = (bf16[2,136,128]{2,1,0:T(8,128)(2,1)S(1)}, bf16[2,136,128]{2,1,0:T(8,128)(2,1)S(1)}, u32[]{:S(2)}, u32[]{:S(2)}) collective-permute-start(bf16[2,136,128]{2,1,0:T(8,128)(2,1)S(1)} %add_convert_fusion.8), channel_id=1, source_target_pairs={{0,8},{4,12},{8,0},{12,4},{16,24},{20,28},{24,16},{28,20},{1,9},{5... | collective-permute-start | bytes 208904 | tf_op jit(solution)/shard_map/ppermute | solution.py:104
  148.5 7.5 %collective-permute-start.29 = (bf16[2,136,128]{2,1,0:T(8,128)(2,1)S(1)}, bf16[2,136,128]{2,1,0:T(8,128)(2,1)S(1)}, u32[]{:S(2)}, u32[]{:S(2)}) collective-permute-start(bf16[2,136,128]{2,1,0:T(8,128)(2,1)S(1)} %add_convert_fusion.4), channel_id=1, source_target_pairs={{0,16},{4,20},{8,24},{12,28},{16,0},{20,4},{24,8},{28,12},{1,17},{... | collective-permute-start | bytes 208904 | tf_op jit(solution)/shard_map/ppermute | solution.py:104
  149.5 7.7 %collective-permute-start.25 = (bf16[2,136,128]{2,1,0:T(8,128)(2,1)S(1)}, bf16[2,136,128]{2,1,0:T(8,128)(2,1)S(1)}, u32[]{:S(2)}, u32[]{:S(2)}) collective-permute-start(bf16[2,136,128]{2,1,0:T(8,128)(2,1)S(1)} %add_convert_fusion.7), channel_id=1, source_target_pairs={{0,16},{4,20},{8,24},{12,28},{16,0},{20,4},{24,8},{28,12},{1,17},{... | collective-permute-start | bytes 208904 | tf_op jit(solution)/shard_map/ppermute | solution.py:104
  156.0 1.3 collective-permute-start.30
  157.2 1.3 collective-permute-start.26
where the time goes:
time: 160 us
  waiting for transfers between devices  65.4 us (41%)
  starting transfers between devices  26.2 us (16%)
  Pallas kernels  24.8 us (16%)
  local copies, waits for them, and re-layouts  15.6 us (10%)
  blocking collectives  14.5 us (9%)
  other arithmetic  9.02 us (6%)
  matrix products  3.12 us (2%)
    ppermute x31, waiting for transfers between devices, swap(): return lax.ppermute(array, axis, [(i, i ^ bit) for i in range(size)])  65.4 us
    ppermute x31, starting transfers between devices, swap(): return lax.ppermute(array, axis, [(i, i ^ bit) for i in range(size)])  26.2 us
    all_gather x1, blocking collectives, square_group(): every = lax.all_gather(tops, 'sp')  14.5 us
    pallas_call x2, Pallas kernels, early_projection(): pl.pallas_call(functools.partial(early_kernel, seq, cut), in_specs=in_vme...  12 us
    pallas_call x4, Pallas kernels, late_memory(): pl.pallas_call(functools.partial(late_kernel, heads, starts, bool(extra),...  11.7 us
    unnamed x26, local copies, waits for them, and re-layouts  7.53 us
    another operation x3, other arithmetic  5.33 us
    squeeze x1, local copies, waits for them, and re-layouts, square_group(): y_a = swap(held[b, :half], 'tp', 2)  3.54 us
  transfers between devices with their start and end apart: 31, of which 15 were waited for; matrix products, arithmetic and copies ran while one was open for 10% of the time, Pallas kernels for 11%

commit v1 on v0

--- a/solution.py
+++ b/solution.py
@@ -216,15 +216,13 @@
 
 
 def add_over_sp(keep, give):
-    halfway = []
     total = keep + swap(give, "sp", 1)
     bit = 2
     while bit < lax.axis_size("sp"):
         wire = lax.optimization_barrier(total.astype(jnp.bfloat16))
-        halfway.append(wire)
         total = wire.astype(jnp.float32) + swap(wire, "sp", bit).astype(jnp.float32)
         bit *= 2
-    return lax.optimization_barrier(total.astype(jnp.bfloat16)), halfway[-1]
+    return lax.optimization_barrier(total.astype(jnp.bfloat16)), wire
 
 
 def read_kernel(layout, place, *refs):
@@ -280,11 +278,16 @@
 
     small = half - HEAD if half % HEAD == 0 and half > HEAD else half
     cuts = [[(0, half)]] * (seq_count - 1) + [[(0, small), (small, half)][: 1 + (small < half)]]
+    if small < half and seq_count > 1:
+        cuts[0] = [(0, HEAD), (HEAD, half)]
 
     def lead(source, b):
         out = []
         for lo, hi in cuts[b]:
-            x_a = swap(source[b, lo:hi], "tp", 1)
+            if out and b == 0:
+                source = tie(source, tip)
+            tip = source[b, lo:hi]
+            x_a = swap(tip, "tp", 1)
             y_b = swap(source[b, half + lo : half + hi], "tp", 2)
             out.append((x_a, y_b))
         return out
@@ -311,7 +314,7 @@
         x_b = swap(held[b, half:], "tp", 1)
         y_a = swap(held[b, :half], "tp", 2)
         if b == 0:
-            shares = lax.optimization_barrier(tuple(shares) + first[0])[: tp - 1]
+            shares = lax.optimization_barrier(tuple(shares) + first[-1])[: tp - 1]
         far.append([])
         for x_a, y_b in first:
             far[b].append((swap(x_a, "tp", 2), swap(y_b, "tp", 1)))
@@ -348,7 +351,8 @@
         before = None
         *sooner, (far_a, far_b) = far[b]
         every = tuple(range(per_head))
-        for (lo, _), (part_a, part_b) in zip(cuts[b], sooner):
+        whole = b < seq_count - 1
+        for (lo, _), (part_a, part_b) in zip(cuts[b], () if whole else sooner):
             part_a, part_b = tie(part_a, *slabs), tie(part_b, *slabs)
             groups = [[(lo, part_a)], [(half + lo, part_b)]]
             (before,) = late_memory(every, groups, before, False, *shared)
@@ -357,9 +361,11 @@
         if ahead:
             far_a, far_b = tie(far_a, *ahead), tie(far_b, *ahead)
         groups = [[(lo, far_a)], [(half + lo, far_b)]]
-        if sooner:
-            groups = [groups[0] + groups[1]]
-        parts = 2 if b == seq_count - 1 else 1
+        if whole:
+            groups = [
+                [(r * half + cut[0], pair[r]) for cut, pair in zip(cuts[b], far[b])] for r in range(2)
+            ]
+        parts = 2 if b == seq_count - 1 and per_head > 1 else 1
         own = []
         for k in range(parts):
             heads = every[per_head * k // parts : per_head * (k + 1) // parts]

time: 160 us -> 158 us (0.988)
  waiting for transfers between devices: 65.4 us -> 53.6 us
  starting transfers between devices: 26.2 us -> 32.2 us
  local copies, waits for them, and re-layouts: 15.6 us -> 17.8 us
  other arithmetic: 9.02 us -> 11.2 us
    ppermute x31 -> x35, waiting for transfers between devices: 65.4 us -> 53.6 us  [swap(): return lax.ppermute(array, axis, [(i, i ^ bit) for i in range(size)])]
    ppermute x31 -> x35, starting transfers between devices: 26.2 us -> 32.2 us  [swap(): return lax.ppermute(array, axis, [(i, i ^ bit) for i in range(size)])]
    unnamed x26 -> x34, local copies, waits for them, and re-layouts: 7.53 us -> 9.45 us
  transfers between devices with their start and end apart: 31 -> 35, of which waited for: 15 -> 14; matrix products, arithmetic and copies ran while one was open for 10% -> 12% of each run, Pallas kernels for 11% -> 11%
where the time goes in v1:
time: 158 us
  waiting for transfers between devices  53.6 us (34%)
  starting transfers between devices  32.2 us (20%)
  Pallas kernels  24.3 us (15%)
  local copies, waits for them, and re-layouts  17.8 us (11%)
  blocking collectives  14.5 us (9%)
  other arithmetic  11.2 us (7%)
  matrix products  3.12 us (2%)
    ppermute x35, waiting for transfers between devices, swap(): return lax.ppermute(array, axis, [(i, i ^ bit) for i in range(size)])  53.6 us
    ppermute x35, starting transfers between devices, swap(): return lax.ppermute(array, axis, [(i, i ^ bit) for i in range(size)])  32.2 us
    all_gather x1, blocking collectives, square_group(): every = lax.all_gather(tops, 'sp')  14.5 us
    pallas_call x2, Pallas kernels, early_projection(): pl.pallas_call(functools.partial(early_kernel, seq, cut), in_specs=in_vme...  11.8 us
    pallas_call x4, Pallas kernels, late_memory(): pl.pallas_call(functools.partial(late_kernel, heads, starts, bool(extra),...  11.4 us
    unnamed x34, local copies, waits for them, and re-layouts  9.45 us
    another operation x3, other arithmetic  5.33 us
    squeeze x1, local copies, waits for them, and re-layouts, square_group(): y_a = swap(held[b, :half], 'tp', 2)  3.55 us
  transfers between devices with their start and end apart: 35, of which 14 were waited for; matrix products, arithmetic and copies ran while one was open for 12% of the time, Pallas kernels for 11%

profile of v1, /device:TPU:0, one launch (start us, length us, event | category | flops | bytes accessed | tf_op | source)
XLA Modules:
  0.0 157.8 jit_solution(1490911026795610215)
XLA Ops:
  0.7 1.0 copy-done
  2.0 3.1 %fusion.21 = f32[4,16,1536]{2,1,0:T(8,128)S(1)} fusion(bf16[4,16,1024]{2,1,0:T(8,128)(2,1)S(1)} %dot_general.5, bf16[1536,1024,1]{1,0,2:T(8,128)(2,1)} %bitcast.72), kind=kOutput, calls=%fused_computation.75 | convolution fusion | flops 201326592 | bytes 3670016 | tf_op jit(solution)/shard_map/dot_general | solution.py:299
  5.1 3.0 %collective-permute-start.10 = (f32[16,1536]{1,0:T(8,128)S(1)}, f32[16,1536]{1,0:T(8,128)S(1)}, u32[]{:S(2)}, u32[]{:S(2)}) collective-permute-start(f32[16,1536]{1,0:T(8,128)S(1)} %get-tuple-element.70), channel_id=1, source_target_pairs={{0,1},{1,0},{2,3},{3,2},{4,5},{5,4},{6,7},{7,6},{8,9},{9,8},{10,11... | collective-permute-start | bytes 294920 | tf_op jit(solution)/shard_map/ppermute | solution.py:104
  8.2 1.5 collective-permute-start.11
  9.7 0.8 slice_bitcast_fusion.10
  10.5 1.0 slice_bitcast_fusion.6
  11.6 1.9 %collective-permute-start.1 = (bf16[256,1024]{1,0:T(8,128)(2,1)}, bf16[256,1024]{1,0:T(8,128)(2,1)S(1)}, u32[]{:S(2)}, u32[]{:S(2)}) collective-permute-start(bf16[256,1024]{1,0:T(8,128)(2,1)} %get-tuple-element.65), channel_id=1, source_target_pairs={{0,1},{1,0},{2,3},{3,2},{4,5},{5,4},{6,7},{7,6},{8,9},{9,8},{10,11... | collective-permute-start | bytes 1572872 | tf_op jit(solution)/shard_map/ppermute | solution.py:104
  13.5 1.5 collective-permute-start.5
  15.1 0.6 fusion.18
  15.9 3.6 %slice_bitcast_fusion = (bf16[384,1024]{1,0:T(8,128)(2,1)}, bf16[384,1024]{1,0:T(8,128)(2,1)}, bf16[384,1024]{1,0:T(8,128)(2,1)}, bf16[384,1024]{1,0:T(8,128)(2,1)}) fusion(bf16[2,768,1024]{2,1,0:T(8,128)(2,1)} %own.3), kind=kLoop, calls=%fused_computation | loop fusion | bytes 6291456 | tf_op jit(solution)/shard_map/squeeze | solution.py:315
  19.5 0.5 collective-permute-start
  20.0 0.6 copy-done.13
  20.7 1.5 collective-permute-start.2
  22.2 0.6 copy-done.14
  23.3 3.3 %collective-permute-done.1.refs_1_ = bf16[256,1024]{1,0:T(8,128)(2,1)S(1)} collective-permute-done((bf16[256,1024]{1,0:T(8,128)(2,1)}, bf16[256,1024]{1,0:T(8,128)(2,1)S(1)}, u32[]{:S(2)}, u32[]{:S(2)}) %collective-permute-start.1) | collective-permute-done | bytes 524320 | tf_op jit(solution)/shard_map/ppermute | solution.py:104
  26.6 2.0 %collective-permute-start.4 = (bf16[128,1024]{1,0:T(8,128)(2,1)}, bf16[128,1024]{1,0:T(8,128)(2,1)}, u32[]{:S(2)}, u32[]{:S(2)}) collective-permute-start(bf16[128,1024]{1,0:T(8,128)(2,1)} %get-tuple-element.66), channel_id=1, source_target_pairs={{0,2},{1,3},{2,0},{3,1},{4,6},{5,7},{6,4},{7,5},{8,10},{9,11},{10,... | collective-permute-start | bytes 786440 | tf_op jit(solution)/shard_map/ppermute | solution.py:104
  28.6 1.7 %fusion.3 = f32[16,1536]{1,0:T(8,128)} fusion(f32[16,1536]{1,0:T(8,128)} %copy-done.14, f32[16,1536]{1,0:T(8,128)} %copy-done.13, f32[16,1536]{1,0:T(8,128)S(1)} %collective-permute-done.10, f32[4,16,1536]{2,1,0:T(8,128)} %copy-done.8, s32[]{:T(128)S(6)} %select_n.56), kind=kLoop, calls=%fused_computation.29 | loop fusion | flops 73728 | bytes 491524 | tf_op jit(solution)/shard_map/add | solution.py:325
  30.2 1.0 reshape.84
  31.2 0.6 copy-done.11
  31.9 1.7 %fusion.16 = (f32[2,4,768]{2,1,0:T(4,128)S(1)}, f32[2,1,4,768]{3,1,2,0:T(1,128)}, f32[2,4,768]{2,1,0:T(4,128)S(1)}) fusion(f32[2,1,4,768]{3,2,1,0:T(4,128)S(1)} %get-tuple-element.74, f32[4]{0:T(128)S(1)} %get-tuple-element.86, f32[2,4,4,768]{3,1,2,0:T(4,128)S(1)} %bitcast.74, f32[2,1,4,768]{3,2,1,0:T(4,128)} %get-tuple-element.75, f32[4]{0:T(128)S(1)} %get-tuple-element.85), kind=kLoop, calls=%fused_computation.71 | loop fusion | flops 122880 | bytes 172064 | tf_op jit(solution)/shard_map/add | solution.py:94
  33.7 4.5 %reduce-window.6 = f32[2,2,4,6,128]{4,3,2,1,0:T(8,128)S(1)} reduce-window(f32[2,2,4,6,128]{4,3,2,1,0:T(8,128)S(1)} %copy.72, f32[]{:T(128)} %constant.60.clone.1), window={size=1x1x1x1x128 pad=0_0x0_0x0_0x0_0x127_0}, to_apply=%region_0.1 | reduce-window | flops 1560576 | bytes 98308 | tf_op jit(solution)/shard_map/reduce-window
  38.4 0.7 reduce-window.9
  39.4 1.1 fusion.9
  40.7 14.5 %all-gather = f32[16,2,2,4]{3,2,1,0:T(2,128)S(1)} all-gather(f32[2,2,2,4]{3,2,1,0:T(2,128)S(1)} %pad_maximum_fusion.2), channel_id=2, replica_groups=mesh['sp'=8,'tp'=4] {'sp'}, dimensions={0}, use_global_device_ids=true | all-gather | bytes 1152 | tf_op jit(solution)/shard_map/all_gather | solution.py:330
  55.6 1.5 collective-permute-start.7
  57.3 0.6 collective-permute-start.9
  57.9 0.6 fusion.15
  58.6 1.5 collective-permute-start.6
  60.1 0.5 collective-permute-start.8
  60.8 2.2 %copy-done.1 = bf16[4096,512]{1,0:T(8,128)(2,1)S(1)} copy-done((bf16[4096,512]{1,0:T(8,128)(2,1)S(1)}, bf16[4096,512]{1,0:T(8,128)(2,1)}, u32[]{:S(2)}) %copy-start.1) | copy-done | bytes 4194328
  62.9 2.2 %copy-done.3 = bf16[4096,512]{1,0:T(8,128)(2,1)S(1)} copy-done((bf16[4096,512]{1,0:T(8,128)(2,1)S(1)}, bf16[4096,512]{1,0:T(8,128)(2,1)}, u32[]{:S(2)}) %copy-start.3) | copy-done | bytes 4194328
  65.1 1.9 %copy-done.6 = bf16[2,768,1024]{2,1,0:T(8,128)(2,1)S(1)} copy-done((bf16[2,768,1024]{2,1,0:T(8,128)(2,1)S(1)}, bf16[2,768,1024]{2,1,0:T(8,128)(2,1)}, u32[]{:S(2)}) %copy-start.6) | copy-done | bytes 3145752
  67.0 6.1 %early.2.acc = f32[4,768,256]{2,1,0:T(8,128)S(1)} custom-call(s32[5]{0:T(128)S(1)} %stack.40.feature, bf16[2,768,1024]{2,1,0:T(8,128)(2,1)S(1)} %copy-done.6, bf16[128,1024]{1,0:T(8,128)(2,1)S(1)} %collective-permute-done.refs_0_, bf16[256,1024]{1,0:T(8,128)(2,1)S(1)} %collective-permute-done.1.refs_1_, ...), custom_call_target="tpu_custom_call" | custom-call | tf_op jit(solution)/shard_map/early/pallas_call | solution.py:142
  73.2 2.3 %collective-permute-done.6.refs_0_ = bf16[128,1024]{1,0:T(8,128)(2,1)S(1)} collective-permute-done((bf16[128,1024]{1,0:T(8,128)(2,1)S(1)}, bf16[128,1024]{1,0:T(8,128)(2,1)S(1)}, u32[]{:S(2)}, u32[]{:S(2)}) %collective-permute-start.6) | collective-permute-done | bytes 262176 | tf_op jit(solution)/shard_map/ppermute | solution.py:104
  75.4 1.4 collective-permute-done.8.refs_2_
  76.9 4.9 %late.4 = (f32[4,136,128]{2,1,0:T(8,128)S(1)}, f32[4,136,128]{2,1,0:T(8,128)S(1)}) custom-call(s32[5]{0:T(128)S(1)} %stack.40.feature, f32[4,768,256]{2,1,0:T(8,128)S(1)} %early.2.acc, bf16[128,1024]{1,0:T(8,128)(2,1)S(1)} %collective-permute-done.6.refs_0_, bf16[256,1024]{1,0:T(8,128)(2,1)} %collective-permute-done.7.refs_1_, ...), custom_call_target="tpu_custom_call" | custom-call | tf_op jit(solution)/shard_map/late/pallas_call | solution.py:204
  82.0 0.6 collective-permute-start.21
  82.6 1.5 collective-permute-start.17
  84.1 0.5 collective-permute-start.20
  84.6 1.6 collective-permute-start.18
  86.2 0.5 collective-permute-start.19
  86.8 16.2 %collective-permute-done.18.refs_1_ = bf16[128,1024]{1,0:T(8,128)(2,1)S(1)} collective-permute-done((bf16[128,1024]{1,0:T(8,128)(2,1)S(1)}, bf16[128,1024]{1,0:T(8,128)(2,1)S(1)}, u32[]{:S(2)}, u32[]{:S(2)}) %collective-permute-start.18) | collective-permute-done | bytes 262176 | tf_op jit(solution)/shard_map/ppermute | solution.py:104
  103.0 1.6 collective-permute-start.14
  104.5 1.5 collective-permute-start.22
  106.6 1.5 collective-permute-done.14
  108.0 1.5 collective-permute-start.24
  109.6 9.7 %collective-permute-done.22.refs_5_ = bf16[128,1024]{1,0:T(8,128)(2,1)S(1)} collective-permute-done((bf16[128,1024]{1,0:T(8,128)(2,1)S(1)}, bf16[128,1024]{1,0:T(8,128)(2,1)S(1)}, u32[]{:S(2)}, u32[]{:S(2)}) %collective-permute-start.22) | collective-permute-done | bytes 262176 | tf_op jit(solution)/shard_map/ppermute | solution.py:104
  119.3 0.6 collective-permute-start.15
  120.4 7.5 %collective-permute-done.15 = bf16[4,136,128]{2,1,0:T(8,128)(2,1)S(1)} collective-permute-done((bf16[4,136,128]{2,1,0:T(8,128)(2,1)S(1)}, bf16[4,136,128]{2,1,0:T(8,128)(2,1)S(1)}, u32[]{:S(2)}, u32[]{:S(2)}) %collective-permute-start.15) | collective-permute-done | bytes 139296 | tf_op jit(solution)/shard_map/ppermute | solution.py:104
  127.9 0.5 collective-permute-start.23
  128.6 5.6 %early.3.acc = f32[4,768,256]{2,1,0:T(8,128)S(1)} custom-call(s32[5]{0:T(128)S(1)} %stack.40.feature, bf16[2,768,1024]{2,1,0:T(8,128)(2,1)S(1)} %copy-done.6, bf16[256,1024]{1,0:T(8,128)(2,1)S(1)} %collective-permute-done.17.refs_0_, bf16[128,1024]{1,0:T(8,128)(2,1)S(1)} %collective-permute-done.18.refs_1_, ...), custom_call_target="tpu_custom_call" | custom-call | tf_op jit(solution)/shard_map/early/pallas_call | solution.py:142
  134.2 3.4 %late.5.refs_5_ = f32[4,272,256]{2,1,0:T(8,128)S(1)} custom-call(s32[5]{0:T(128)S(1)} %stack.40.feature, f32[4,768,256]{2,1,0:T(8,128)S(1)} %early.3.acc, bf16[256,1024]{1,0:T(8,128)(2,1)S(1)} %collective-permute-done.24.refs_0_, bf16[256,1024]{1,0:T(8,128)(2,1)S(1)} %collective-permute-done.25.refs_1_, bf16[4096,512]{1,0:T(8,128)(2,1)S(1)} %copy-done.2, ...), custom_call_target="tpu_custom_call" | custom-call | tf_op jit(solution)/shard_map/late/pallas_call | solution.py:204
  137.6 1.6 %late.7 = (f32[2,136,128]{2,1,0:T(8,128)S(1)}, f32[2,136,128]{2,1,0:T(8,128)S(1)}) custom-call(s32[5]{0:T(128)S(1)} %stack.40.feature, f32[4,768,256]{2,1,0:T(8,128)S(1)} %early.3.acc, bf16[128,1024]{1,0:T(8,128)(2,1)S(1)} %collective-permute-done.23.refs_0_, bf16[128,1024]{1,0:T(8,128)(2,1)S(1)} %collective-permute-done.26.refs_1_, ...), custom_call_target="tpu_custom_call" | custom-call | tf_op jit(solution)/shard_map/late/pallas_call | solution.py:204
  139.2 0.6 collective-permute-start.31
  139.8 1.6 %late.6 = (f32[2,136,128]{2,1,0:T(8,128)S(1)}, f32[2,136,128]{2,1,0:T(8,128)S(1)}) custom-call(s32[5]{0:T(128)S(1)} %stack.40.feature, f32[4,768,256]{2,1,0:T(8,128)S(1)} %early.3.acc, bf16[128,1024]{1,0:T(8,128)(2,1)S(1)} %collective-permute-done.23.refs_0_, bf16[128,1024]{1,0:T(8,128)(2,1)S(1)} %collective-permute-done.26.refs_1_, ...), custom_call_target="tpu_custom_call" | custom-call | tf_op jit(solution)/shard_map/late/pallas_call | solution.py:204
  141.6 1.2 collective-permute-done.27
  142.8 0.9 collective-permute-start.28
  143.7 2.9 %collective-permute-done.32 = bf16[2,136,128]{2,1,0:T(8,128)(2,1)S(1)} collective-permute-done((bf16[2,136,128]{2,1,0:T(8,128)(2,1)S(1)}, bf16[2,136,128]{2,1,0:T(8,128)(2,1)S(1)}, u32[]{:S(2)}, u32[]{:S(2)}) %collective-permute-start.32) | collective-permute-done | bytes 69664 | tf_op jit(solution)/shard_map/ppermute | solution.py:104
  146.8 0.8 collective-permute-done.28
  147.6 2.1 %collective-permute-start.29 = (bf16[2,136,128]{2,1,0:T(8,128)(2,1)S(1)}, bf16[2,136,128]{2,1,0:T(8,128)(2,1)S(1)}, u32[]{:S(2)}, u32[]{:S(2)}) collective-permute-start(bf16[2,136,128]{2,1,0:T(8,128)(2,1)S(1)} %add_convert_fusion.7), channel_id=1, source_target_pairs={{0,16},{4,20},{8,24},{12,28},{16,0},{20,4},{24,8},{28,12},{1,17},{... | collective-permute-start | bytes 208904 | tf_op jit(solution)/shard_map/ppermute | solution.py:104
  149.7 4.4 %collective-permute-done.33 = bf16[2,136,128]{2,1,0:T(8,128)(2,1)S(1)} collective-permute-done((bf16[2,136,128]{2,1,0:T(8,128)(2,1)S(1)}, bf16[2,136,128]{2,1,0:T(8,128)(2,1)S(1)}, u32[]{:S(2)}, u32[]{:S(2)}) %collective-permute-start.33) | collective-permute-done | bytes 69664 | tf_op jit(solution)/shard_map/ppermute | solution.py:104
  154.2 1.1 collective-permute-done.29
  155.5 1.2 collective-permute-done.30.refs_3_
  156.6 1.2 read.1
  (103 shorter events, 4.8 us)
Async XLA Ops:
  0.6 1.0 copy-start
  1.9 7.8 %copy-start.5 = (bf16[2,768,1024]{2,1,0:T(8,128)(2,1)S(1)}, bf16[2,768,1024]{2,1,0:T(8,128)(2,1)}, u32[]{:S(2)}) copy-start(bf16[2,768,1024]{2,1,0:T(8,128)(2,1)} %own.3) | copy-start | bytes 9437188
  1.9 13.1 %copy-start.12 = (f32[2,4,4,768]{3,2,1,0:T(4,128)S(1)}, f32[2,4,4,768]{3,2,1,0:T(4,128)}, u32[]{:S(2)}) copy-start(f32[2,4,4,768]{3,2,1,0:T(4,128)} %param.12) | copy-start | bytes 294916
  2.0 13.7 %copy-start.15 = (f32[2,16]{1,0:T(2,128)S(1)}, f32[2,16]{1,0:T(2,128)}, u32[]{:S(2)}) copy-start(f32[2,16]{1,0:T(2,128)} %param.11) | copy-start | bytes 388
  5.1 8.4 %copy-start.8 = (f32[4,16,1536]{2,1,0:T(8,128)}, f32[4,16,1536]{2,1,0:T(8,128)S(1)}, u32[]{:S(2)}) copy-start(f32[4,16,1536]{2,1,0:T(8,128)S(1)} %fusion.21) | copy-start | bytes 1179652
  5.1 14.4 %collective-permute-start.10 = (f32[16,1536]{1,0:T(8,128)S(1)}, f32[16,1536]{1,0:T(8,128)S(1)}, u32[]{:S(2)}, u32[]{:S(2)}) collective-permute-start(f32[16,1536]{1,0:T(8,128)S(1)} %get-tuple-element.70), channel_id=1, source_target_pairs={{0,1},{1,0},{2,3},{3,2},{4,5},{5,4},{6,7},{7,6},{8,9},{9,8},{10,11... | collective-permute-start | bytes 294920 | tf_op jit(solution)/shard_map/ppermute | solution.py:104
  8.2 11.9 %collective-permute-start.11 = (f32[16,1536]{1,0:T(8,128)S(1)}, f32[16,1536]{1,0:T(8,128)S(1)}, u32[]{:S(2)}, u32[]{:S(2)}) collective-permute-start(f32[16,1536]{1,0:T(8,128)S(1)} %get-tuple-element.69), channel_id=1, source_target_pairs={{0,2},{1,3},{2,0},{3,1},{4,6},{5,7},{6,4},{7,5},{8,10},{9,11},{10,... | collective-permute-start | bytes 294920 | tf_op jit(solution)/shard_map/ppermute | solution.py:104
  9.7 12.5 %collective-permute-start.12 = (f32[16,1536]{1,0:T(8,128)S(1)}, f32[16,1536]{1,0:T(8,128)S(1)}, u32[]{:S(2)}, u32[]{:S(2)}) collective-permute-start(f32[16,1536]{1,0:T(8,128)S(1)} %get-tuple-element.68), channel_id=1, source_target_pairs={{0,3},{1,2},{2,1},{3,0},{4,7},{5,6},{6,5},{7,4},{8,11},{9,10},{10,... | collective-permute-start | bytes 294920 | tf_op jit(solution)/shard_map/ppermute | solution.py:104
  11.6 15.0 %collective-permute-start.1 = (bf16[256,1024]{1,0:T(8,128)(2,1)}, bf16[256,1024]{1,0:T(8,128)(2,1)S(1)}, u32[]{:S(2)}, u32[]{:S(2)}) collective-permute-start(bf16[256,1024]{1,0:T(8,128)(2,1)} %get-tuple-element.65), channel_id=1, source_target_pairs={{0,1},{1,0},{2,3},{3,2},{4,5},{5,4},{6,7},{7,6},{8,9},{9,8},{10,11... | collective-permute-start | bytes 1572872 | tf_op jit(solution)/shard_map/ppermute | solution.py:104
  13.5 15.0 %collective-permute-start.5 = (bf16[256,1024]{1,0:T(8,128)(2,1)}, bf16[256,1024]{1,0:T(8,128)(2,1)S(1)}, u32[]{:S(2)}, u32[]{:S(2)}) collective-permute-start(bf16[256,1024]{1,0:T(8,128)(2,1)} %get-tuple-element.64), channel_id=1, source_target_pairs={{0,2},{1,3},{2,0},{3,1},{4,6},{5,7},{6,4},{7,5},{8,10},{9,11},{10,... | collective-permute-start | bytes 1572872 | tf_op jit(solution)/shard_map/ppermute | solution.py:104
  19.5 37.8 %collective-permute-start = (bf16[128,1024]{1,0:T(8,128)(2,1)}, bf16[128,1024]{1,0:T(8,128)(2,1)S(1)}, u32[]{:S(2)}, u32[]{:S(2)}) collective-permute-start(bf16[128,1024]{1,0:T(8,128)(2,1)} %get-tuple-element.67), channel_id=1, source_target_pairs={{0,1},{1,0},{2,3},{3,2},{4,5},{5,4},{6,7},{7,6},{8,9},{9,8},{10,11... | collective-permute-start | bytes 786440 | tf_op jit(solution)/shard_map/ppermute | solution.py:104
  20.0 0.6 copy-start.13
  20.7 39.4 %collective-permute-start.2 = (bf16[384,1024]{1,0:T(8,128)(2,1)}, bf16[384,1024]{1,0:T(8,128)(2,1)S(1)}, u32[]{:S(2)}, u32[]{:S(2)}) collective-permute-start(bf16[384,1024]{1,0:T(8,128)(2,1)} %get-tuple-element.63), channel_id=1, source_target_pairs={{0,1},{1,0},{2,3},{3,2},{4,5},{5,4},{6,7},{7,6},{8,9},{9,8},{10,11... | collective-permute-start | bytes 2359304 | tf_op jit(solution)/shard_map/ppermute | solution.py:104
  22.2 0.7 copy-start.14
  22.8 37.9 %collective-permute-start.3 = (bf16[384,1024]{1,0:T(8,128)(2,1)}, bf16[384,1024]{1,0:T(8,128)(2,1)S(1)}, u32[]{:S(2)}, u32[]{:S(2)}) collective-permute-start(bf16[384,1024]{1,0:T(8,128)(2,1)} %get-tuple-element.62), channel_id=1, source_target_pairs={{0,2},{1,3},{2,0},{3,1},{4,6},{5,7},{6,4},{7,5},{8,10},{9,11},{10,... | collective-permute-start | bytes 2359304 | tf_op jit(solution)/shard_map/ppermute | solution.py:104
  26.6 32.0 %collective-permute-start.4 = (bf16[128,1024]{1,0:T(8,128)(2,1)}, bf16[128,1024]{1,0:T(8,128)(2,1)}, u32[]{:S(2)}, u32[]{:S(2)}) collective-permute-start(bf16[128,1024]{1,0:T(8,128)(2,1)} %get-tuple-element.66), channel_id=1, source_target_pairs={{0,2},{1,3},{2,0},{3,1},{4,6},{5,7},{6,4},{7,5},{8,10},{9,11},{10,... | collective-permute-start | bytes 786440 | tf_op jit(solution)/shard_map/ppermute | solution.py:104
  31.2 0.6 copy-start.11
  55.6 21.2 %collective-permute-start.7 = (bf16[256,1024]{1,0:T(8,128)(2,1)S(1)}, bf16[256,1024]{1,0:T(8,128)(2,1)}, u32[]{:S(2)}, u32[]{:S(2)}) collective-permute-start(bf16[256,1024]{1,0:T(8,128)(2,1)S(1)} %collective-permute-done.1.refs_1_), channel_id=1, source_target_pairs={{0,2},{1,3},{2,0},{3,1},{4,6},{5,7},{6,4},{7,5},{8,10},{9,11},{10,... | collective-permute-start | bytes 1572872 | tf_op jit(solution)/shard_map/ppermute | solution.py:104
  57.3 19.6 %collective-permute-start.9 = (bf16[256,1024]{1,0:T(8,128)(2,1)S(1)}, bf16[256,1024]{1,0:T(8,128)(2,1)}, u32[]{:S(2)}, u32[]{:S(2)}) collective-permute-start(bf16[256,1024]{1,0:T(8,128)(2,1)S(1)} %collective-permute-done.5.refs_5_), channel_id=1, source_target_pairs={{0,1},{1,0},{2,3},{3,2},{4,5},{5,4},{6,7},{7,6},{8,9},{9,8},{10,11... | collective-permute-start | bytes 1572872 | tf_op jit(solution)/shard_map/ppermute | solution.py:104
  58.6 16.9 %collective-permute-start.6 = (bf16[128,1024]{1,0:T(8,128)(2,1)S(1)}, bf16[128,1024]{1,0:T(8,128)(2,1)S(1)}, u32[]{:S(2)}, u32[]{:S(2)}) collective-permute-start(bf16[128,1024]{1,0:T(8,128)(2,1)S(1)} %collective-permute-done.refs_0_), channel_id=1, source_target_pairs={{0,2},{1,3},{2,0},{3,1},{4,6},{5,7},{6,4},{7,5},{8,10},{9,11},{10,... | collective-permute-start | bytes 786440 | tf_op jit(solution)/shard_map/ppermute | solution.py:104
  60.1 16.8 %collective-permute-start.8 = (bf16[128,1024]{1,0:T(8,128)(2,1)}, bf16[128,1024]{1,0:T(8,128)(2,1)S(1)}, u32[]{:S(2)}, u32[]{:S(2)}) collective-permute-start(bf16[128,1024]{1,0:T(8,128)(2,1)} %collective-permute-done.4.refs_4_), channel_id=1, source_target_pairs={{0,1},{1,0},{2,3},{3,2},{4,5},{5,4},{6,7},{7,6},{8,9},{9,8},{10,11... | collective-permute-start | bytes 786440 | tf_op jit(solution)/shard_map/ppermute | solution.py:104
  60.7 2.2 %copy-start.1 = (bf16[4096,512]{1,0:T(8,128)(2,1)S(1)}, bf16[4096,512]{1,0:T(8,128)(2,1)}, u32[]{:S(2)}) copy-start(bf16[4096,512]{1,0:T(8,128)(2,1)} %refs_2_.5) | copy-start | bytes 12582916
  62.9 2.2 %copy-start.3 = (bf16[4096,512]{1,0:T(8,128)(2,1)S(1)}, bf16[4096,512]{1,0:T(8,128)(2,1)}, u32[]{:S(2)}) copy-start(bf16[4096,512]{1,0:T(8,128)(2,1)} %refs_3_.5) | copy-start | bytes 12582916
  65.1 1.9 %copy-start.6 = (bf16[2,768,1024]{2,1,0:T(8,128)(2,1)S(1)}, bf16[2,768,1024]{2,1,0:T(8,128)(2,1)}, u32[]{:S(2)}) copy-start(bf16[2,768,1024]{2,1,0:T(8,128)(2,1)} %own.3) | copy-start | bytes 9437188
  67.0 9.9 %copy-start.2 = (bf16[4096,512]{1,0:T(8,128)(2,1)S(1)}, bf16[4096,512]{1,0:T(8,128)(2,1)}, u32[]{:S(2)}) copy-start(bf16[4096,512]{1,0:T(8,128)(2,1)} %refs_2_.5) | copy-start | bytes 12582916
  67.0 9.9 %copy-start.4 = (bf16[4096,512]{1,0:T(8,128)(2,1)S(1)}, bf16[4096,512]{1,0:T(8,128)(2,1)}, u32[]{:S(2)}) copy-start(bf16[4096,512]{1,0:T(8,128)(2,1)} %refs_3_.5) | copy-start | bytes 12582916
  76.9 7.2 %copy-start.10 = (bf16[384,1024]{1,0:T(8,128)(2,1)S(1)}, bf16[384,1024]{1,0:T(8,128)(2,1)}, u32[]{:S(2)}) copy-start(bf16[384,1024]{1,0:T(8,128)(2,1)} %get-tuple-element.60) | copy-start | bytes 2359300
  81.8 4.4 %copy-start.9 = (bf16[384,1024]{1,0:T(8,128)(2,1)S(1)}, bf16[384,1024]{1,0:T(8,128)(2,1)}, u32[]{:S(2)}) copy-start(bf16[384,1024]{1,0:T(8,128)(2,1)} %get-tuple-element.61) | copy-start | bytes 2359300
  81.8 4.4 %collective-permute-start.13 = (f32[4,136,128]{2,1,0:T(8,128)S(1)}, f32[4,136,128]{2,1,0:T(8,128)S(1)}, u32[]{:S(2)}, u32[]{:S(2)}) collective-permute-start(f32[4,136,128]{2,1,0:T(8,128)S(1)} %get-tuple-element.34), channel_id=1, source_target_pairs={{0,4},{4,0},{8,12},{12,8},{16,20},{20,16},{24,28},{28,24},{1,5},{5... | collective-permute-start | bytes 835592 | tf_op jit(solution)/shard_map/ppermute | solution.py:104
  82.0 22.6 %collective-permute-start.21 = (bf16[256,1024]{1,0:T(8,128)(2,1)S(1)}, bf16[256,1024]{1,0:T(8,128)(2,1)S(1)}, u32[]{:S(2)}, u32[]{:S(2)}) collective-permute-start(bf16[256,1024]{1,0:T(8,128)(2,1)S(1)} %get-tuple-element.58), channel_id=1, source_target_pairs={{0,2},{1,3},{2,0},{3,1},{4,6},{5,7},{6,4},{7,5},{8,10},{9,11},{10,... | collective-permute-start | bytes 1572872 | tf_op jit(solution)/shard_map/ppermute | solution.py:104
  82.6 23.5 %collective-permute-start.17 = (bf16[256,1024]{1,0:T(8,128)(2,1)S(1)}, bf16[256,1024]{1,0:T(8,128)(2,1)S(1)}, u32[]{:S(2)}, u32[]{:S(2)}) collective-permute-start(bf16[256,1024]{1,0:T(8,128)(2,1)S(1)} %get-tuple-element.59), channel_id=1, source_target_pairs={{0,1},{1,0},{2,3},{3,2},{4,5},{5,4},{6,7},{7,6},{8,9},{9,8},{10,11... | collective-permute-start | bytes 1572872 | tf_op jit(solution)/shard_map/ppermute | solution.py:104
  84.1 35.8 %collective-permute-start.20 = (bf16[384,1024]{1,0:T(8,128)(2,1)S(1)}, bf16[384,1024]{1,0:T(8,128)(2,1)S(1)}, u32[]{:S(2)}, u32[]{:S(2)}) collective-permute-start(bf16[384,1024]{1,0:T(8,128)(2,1)S(1)} %copy-done.10), channel_id=1, source_target_pairs={{0,2},{1,3},{2,0},{3,1},{4,6},{5,7},{6,4},{7,5},{8,10},{9,11},{10,... | collective-permute-start | bytes 2359304 | tf_op jit(solution)/shard_map/ppermute | solution.py:104
  84.6 18.3 %collective-permute-start.18 = (bf16[128,1024]{1,0:T(8,128)(2,1)S(1)}, bf16[128,1024]{1,0:T(8,128)(2,1)S(1)}, u32[]{:S(2)}, u32[]{:S(2)}) collective-permute-start(bf16[128,1024]{1,0:T(8,128)(2,1)S(1)} %get-tuple-element.57), channel_id=1, source_target_pairs={{0,1},{1,0},{2,3},{3,2},{4,5},{5,4},{6,7},{7,6},{8,9},{9,8},{10,11... | collective-permute-start | bytes 786440 | tf_op jit(solution)/shard_map/ppermute | solution.py:104
  86.2 42.3 %collective-permute-start.19 = (bf16[384,1024]{1,0:T(8,128)(2,1)S(1)}, bf16[384,1024]{1,0:T(8,128)(2,1)S(1)}, u32[]{:S(2)}, u32[]{:S(2)}) collective-permute-start(bf16[384,1024]{1,0:T(8,128)(2,1)S(1)} %copy-done.9), channel_id=1, source_target_pairs={{0,1},{1,0},{2,3},{3,2},{4,5},{5,4},{6,7},{7,6},{8,9},{9,8},{10,11... | collective-permute-start | bytes 2359304 | tf_op jit(solution)/shard_map/ppermute | solution.py:104
  103.0 5.1 %collective-permute-start.14 = (bf16[4,136,128]{2,1,0:T(8,128)(2,1)S(1)}, bf16[4,136,128]{2,1,0:T(8,128)(2,1)S(1)}, u32[]{:S(2)}, u32[]{:S(2)}) collective-permute-start(bf16[4,136,128]{2,1,0:T(8,128)(2,1)S(1)} %add_convert_fusion.2), channel_id=1, source_target_pairs={{0,8},{4,12},{8,0},{12,4},{16,24},{20,28},{24,16},{28,20},{1,9},{5... | collective-permute-start | bytes 417800 | tf_op jit(solution)/shard_map/ppermute | solution.py:104
  104.5 14.8 %collective-permute-start.22 = (bf16[128,1024]{1,0:T(8,128)(2,1)S(1)}, bf16[128,1024]{1,0:T(8,128)(2,1)S(1)}, u32[]{:S(2)}, u32[]{:S(2)}) collective-permute-start(bf16[128,1024]{1,0:T(8,128)(2,1)S(1)} %get-tuple-element.56), channel_id=1, source_target_pairs={{0,2},{1,3},{2,0},{3,1},{4,6},{5,7},{6,4},{7,5},{8,10},{9,11},{10,... | collective-permute-start | bytes 786440 | tf_op jit(solution)/shard_map/ppermute | solution.py:104
  106.0 28.2 %collective-permute-start.25 = (bf16[256,1024]{1,0:T(8,128)(2,1)S(1)}, bf16[256,1024]{1,0:T(8,128)(2,1)S(1)}, u32[]{:S(2)}, u32[]{:S(2)}) collective-permute-start(bf16[256,1024]{1,0:T(8,128)(2,1)S(1)} %collective-permute-done.21.refs_4_), channel_id=1, source_target_pairs={{0,1},{1,0},{2,3},{3,2},{4,5},{5,4},{6,7},{7,6},{8,9},{9,8},{10,11... | collective-permute-start | bytes 1572872 | tf_op jit(solution)/shard_map/ppermute | solution.py:104
  108.0 26.2 %collective-permute-start.24 = (bf16[256,1024]{1,0:T(8,128)(2,1)S(1)}, bf16[256,1024]{1,0:T(8,128)(2,1)S(1)}, u32[]{:S(2)}, u32[]{:S(2)}) collective-permute-start(bf16[256,1024]{1,0:T(8,128)(2,1)S(1)} %collective-permute-done.17.refs_0_), channel_id=1, source_target_pairs={{0,2},{1,3},{2,0},{3,1},{4,6},{5,7},{6,4},{7,5},{8,10},{9,11},{10,... | collective-permute-start | bytes 1572872 | tf_op jit(solution)/shard_map/ppermute | solution.py:104
  119.3 8.6 %collective-permute-start.15 = (bf16[4,136,128]{2,1,0:T(8,128)(2,1)S(1)}, bf16[4,136,128]{2,1,0:T(8,128)(2,1)S(1)}, u32[]{:S(2)}, u32[]{:S(2)}) collective-permute-start(bf16[4,136,128]{2,1,0:T(8,128)(2,1)S(1)} %add_convert_fusion.1), channel_id=1, source_target_pairs={{0,16},{4,20},{8,24},{12,28},{16,0},{20,4},{24,8},{28,12},{1,17},{... | collective-permute-start | bytes 417800 | tf_op jit(solution)/shard_map/ppermute | solution.py:104
  119.9 17.7 %collective-permute-start.26 = (bf16[128,1024]{1,0:T(8,128)(2,1)S(1)}, bf16[128,1024]{1,0:T(8,128)(2,1)S(1)}, u32[]{:S(2)}, u32[]{:S(2)}) collective-permute-start(bf16[128,1024]{1,0:T(8,128)(2,1)S(1)} %collective-permute-done.22.refs_5_), channel_id=1, source_target_pairs={{0,1},{1,0},{2,3},{3,2},{4,5},{5,4},{6,7},{7,6},{8,9},{9,8},{10,11... | collective-permute-start | bytes 786440 | tf_op jit(solution)/shard_map/ppermute | solution.py:104
  127.9 9.7 %collective-permute-start.23 = (bf16[128,1024]{1,0:T(8,128)(2,1)S(1)}, bf16[128,1024]{1,0:T(8,128)(2,1)S(1)}, u32[]{:S(2)}, u32[]{:S(2)}) collective-permute-start(bf16[128,1024]{1,0:T(8,128)(2,1)S(1)} %collective-permute-done.18.refs_1_), channel_id=1, source_target_pairs={{0,2},{1,3},{2,0},{3,1},{4,6},{5,7},{6,4},{7,5},{8,10},{9,11},{10,... | collective-permute-start | bytes 786440 | tf_op jit(solution)/shard_map/ppermute | solution.py:104
  128.5 5.7 %collective-permute-start.16 = (bf16[4,136,128]{2,1,0:T(8,128)(2,1)S(1)}, bf16[4,136,128]{2,1,0:T(8,128)(2,1)S(1)}, u32[]{:S(2)}, u32[]{:S(2)}) collective-permute-start(bf16[4,136,128]{2,1,0:T(8,128)(2,1)S(1)} %add_convert_fusion.refs_0_), channel_id=1, source_target_pairs={{0,4},{4,0},{8,12},{12,8},{16,20},{20,16},{24,28},{28,24},{1,5},{5... | collective-permute-start | bytes 417800 | tf_op jit(solution)/shard_map/ppermute | solution.py:104
  139.2 17.4 %copy-start.7 = (bf16[2,128,512]{2,1,0:T(8,128)(2,1)S(1)}, bf16[2,128,512]{2,1,0:T(8,128)(2,1)}, u32[]{:S(2)}) copy-start(bf16[2,128,512]{2,1,0:T(8,128)(2,1)} %refs_6_.5) | copy-start | bytes 786436
  139.2 2.2 %collective-permute-start.31 = (f32[2,136,128]{2,1,0:T(8,128)S(1)}, f32[2,136,128]{2,1,0:T(8,128)S(1)}, u32[]{:S(2)}, u32[]{:S(2)}) collective-permute-start(f32[2,136,128]{2,1,0:T(8,128)S(1)} %get-tuple-element.48), channel_id=1, source_target_pairs={{0,4},{4,0},{8,12},{12,8},{16,20},{20,16},{24,28},{28,24},{1,5},{5... | collective-permute-start | bytes 417800 | tf_op jit(solution)/shard_map/ppermute | solution.py:104
  141.4 1.4 collective-permute-start.27
  141.5 5.1 %collective-permute-start.32 = (bf16[2,136,128]{2,1,0:T(8,128)(2,1)S(1)}, bf16[2,136,128]{2,1,0:T(8,128)(2,1)S(1)}, u32[]{:S(2)}, u32[]{:S(2)}) collective-permute-start(bf16[2,136,128]{2,1,0:T(8,128)(2,1)S(1)} %add_convert_fusion.5), channel_id=1, source_target_pairs={{0,8},{4,12},{8,0},{12,4},{16,24},{20,28},{24,16},{28,20},{1,9},{5... | collective-permute-start | bytes 208904 | tf_op jit(solution)/shard_map/ppermute | solution.py:104
  142.8 4.8 %collective-permute-start.28 = (bf16[2,136,128]{2,1,0:T(8,128)(2,1)S(1)}, bf16[2,136,128]{2,1,0:T(8,128)(2,1)S(1)}, u32[]{:S(2)}, u32[]{:S(2)}) collective-permute-start(bf16[2,136,128]{2,1,0:T(8,128)(2,1)S(1)} %add_convert_fusion.8), channel_id=1, source_target_pairs={{0,8},{4,12},{8,0},{12,4},{16,24},{20,28},{24,16},{28,20},{1,9},{5... | collective-permute-start | bytes 208904 | tf_op jit(solution)/shard_map/ppermute | solution.py:104
  146.6 7.5 %collective-permute-start.33 = (bf16[2,136,128]{2,1,0:T(8,128)(2,1)S(1)}, bf16[2,136,128]{2,1,0:T(8,128)(2,1)S(1)}, u32[]{:S(2)}, u32[]{:S(2)}) collective-permute-start(bf16[2,136,128]{2,1,0:T(8,128)(2,1)S(1)} %add_convert_fusion.4), channel_id=1, source_target_pairs={{0,16},{4,20},{8,24},{12,28},{16,0},{20,4},{24,8},{28,12},{1,17},{... | collective-permute-start | bytes 208904 | tf_op jit(solution)/shard_map/ppermute | solution.py:104
  147.6 7.7 %collective-permute-start.29 = (bf16[2,136,128]{2,1,0:T(8,128)(2,1)S(1)}, bf16[2,136,128]{2,1,0:T(8,128)(2,1)S(1)}, u32[]{:S(2)}, u32[]{:S(2)}) collective-permute-start(bf16[2,136,128]{2,1,0:T(8,128)(2,1)S(1)} %add_convert_fusion.7), channel_id=1, source_target_pairs={{0,16},{4,20},{8,24},{12,28},{16,0},{20,4},{24,8},{28,12},{1,17},{... | collective-permute-start | bytes 208904 | tf_op jit(solution)/shard_map/ppermute | solution.py:104
  154.1 1.3 collective-permute-start.34
  155.3 1.3 collective-permute-start.30

commit v2 on v1

--- a/solution.py
+++ b/solution.py
@@ -104,6 +104,12 @@
     return lax.ppermute(array, axis, [(i, i ^ bit) for i in range(size)])
 
 
+def norm_scales():
+    count = SLAB - HEAD
+    row = lax.broadcasted_iota(jnp.int32, (count, HEAD), 0)
+    return jnp.exp2(row.astype(jnp.float32) / count)
+
+
 def head_weights(w_key, w_value, block, width, h):
     rows = pl.ds(pl.multiple_of(block * width, width), width)
     cols = slice(h * HEAD, (h + 1) * HEAD)
@@ -185,7 +191,7 @@
         for j in range(2):
             norm = total[2 * HEAD + j : 2 * HEAD + j + 1, :HEAD]
             norm = norm + total[2 * HEAD + 8 + j : 2 * HEAD + 8 + j + 1, :HEAD]
-            norm = jnp.broadcast_to(norm, (SLAB - HEAD, HEAD))
+            norm = norm * norm_scales()
             slabs.append(jnp.concatenate([total[j * HEAD : (j + 1) * HEAD, HEAD:], norm], axis=0))
         first = feature[4] == 0
         keep, give = rest[-2:]
@@ -235,7 +241,8 @@
         j = core if i == 0 else 1 - core
         for k, h in enumerate(heads):
             matrix_out[b, j, h] = slab[k, :HEAD, :]
-            norm_out[b, j, h : h + 1] = slab[k, HEAD:, :].astype(jnp.float32)[0:1]
+            norm = slab[k, HEAD:, :].astype(jnp.float32) / norm_scales()
+            norm_out[b, j, h : h + 1] = jnp.mean(norm, axis=0, keepdims=True)
     for b in range(seq_count):
         for h in range(per_head):
             q = query[b, :, h * HEAD : (h + 1) * HEAD]

time: 158 us -> 158 us (level)
  no operation moved by 1% of the time
where the time goes in v2:
time: 158 us
  waiting for transfers between devices  53.6 us (34%)
  starting transfers between devices  32.2 us (20%)
  Pallas kernels  24.3 us (15%)
  local copies, waits for them, and re-layouts  17.8 us (11%)
  blocking collectives  14.5 us (9%)
  other arithmetic  11.2 us (7%)
  matrix products  3.12 us (2%)
    ppermute x35, waiting for transfers between devices, swap(): return lax.ppermute(array, axis, [(i, i ^ bit) for i in range(size)])  53.6 us
    ppermute x35, starting transfers between devices, swap(): return lax.ppermute(array, axis, [(i, i ^ bit) for i in range(size)])  32.2 us
    all_gather x1, blocking collectives, square_group(): every = lax.all_gather(tops, 'sp')  14.5 us
    pallas_call x2, Pallas kernels, early_projection(): pl.pallas_call(functools.partial(early_kernel, seq, cut), in_specs=in_vme...  11.8 us
    pallas_call x4, Pallas kernels, late_memory(): pl.pallas_call(functools.partial(late_kernel, heads, starts, bool(extra),...  11.4 us
    unnamed x34, local copies, waits for them, and re-layouts  9.45 us
    another operation x3, other arithmetic  5.33 us
    squeeze x1, local copies, waits for them, and re-layouts, square_group(): y_a = swap(held[b, :half], 'tp', 2)  3.55 us
  transfers between devices with their start and end apart: 35, of which 14 were waited for; matrix products, arithmetic and copies ran while one was open for 12% of the time, Pallas kernels for 11%

profile of v2, /device:TPU:0, one launch (start us, length us, event | category | flops | bytes accessed | tf_op | source)
XLA Modules:
  0.0 157.8 jit_solution(1382368288082729848)
XLA Ops:
  0.7 1.0 copy-done
  2.0 3.1 %fusion.21 = f32[4,16,1536]{2,1,0:T(8,128)S(1)} fusion(bf16[4,16,1024]{2,1,0:T(8,128)(2,1)S(1)} %dot_general.5, bf16[1536,1024,1]{1,0,2:T(8,128)(2,1)} %bitcast.72), kind=kOutput, calls=%fused_computation.75 | convolution fusion | flops 201326592 | bytes 3670016 | tf_op jit(solution)/shard_map/dot_general | solution.py:306
  5.1 3.0 %collective-permute-start.10 = (f32[16,1536]{1,0:T(8,128)S(1)}, f32[16,1536]{1,0:T(8,128)S(1)}, u32[]{:S(2)}, u32[]{:S(2)}) collective-permute-start(f32[16,1536]{1,0:T(8,128)S(1)} %get-tuple-element.70), channel_id=1, source_target_pairs={{0,1},{1,0},{2,3},{3,2},{4,5},{5,4},{6,7},{7,6},{8,9},{9,8},{10,11... | collective-permute-start | bytes 294920 | tf_op jit(solution)/shard_map/ppermute | solution.py:104
  8.2 1.5 collective-permute-start.11
  9.7 0.8 slice_bitcast_fusion.10
  10.5 1.0 slice_bitcast_fusion.6
  11.6 1.9 %collective-permute-start.1 = (bf16[256,1024]{1,0:T(8,128)(2,1)}, bf16[256,1024]{1,0:T(8,128)(2,1)S(1)}, u32[]{:S(2)}, u32[]{:S(2)}) collective-permute-start(bf16[256,1024]{1,0:T(8,128)(2,1)} %get-tuple-element.65), channel_id=1, source_target_pairs={{0,1},{1,0},{2,3},{3,2},{4,5},{5,4},{6,7},{7,6},{8,9},{9,8},{10,11... | collective-permute-start | bytes 1572872 | tf_op jit(solution)/shard_map/ppermute | solution.py:104
  13.5 1.5 collective-permute-start.5
  15.1 0.6 fusion.18
  15.9 3.6 %slice_bitcast_fusion = (bf16[384,1024]{1,0:T(8,128)(2,1)}, bf16[384,1024]{1,0:T(8,128)(2,1)}, bf16[384,1024]{1,0:T(8,128)(2,1)}, bf16[384,1024]{1,0:T(8,128)(2,1)}) fusion(bf16[2,768,1024]{2,1,0:T(8,128)(2,1)} %own.3), kind=kLoop, calls=%fused_computation | loop fusion | bytes 6291456 | tf_op jit(solution)/shard_map/squeeze | solution.py:322
  19.5 0.5 collective-permute-start
  20.0 0.6 copy-done.13
  20.7 1.5 collective-permute-start.2
  22.2 0.6 copy-done.14
  23.3 3.3 %collective-permute-done.1.refs_1_ = bf16[256,1024]{1,0:T(8,128)(2,1)S(1)} collective-permute-done((bf16[256,1024]{1,0:T(8,128)(2,1)}, bf16[256,1024]{1,0:T(8,128)(2,1)S(1)}, u32[]{:S(2)}, u32[]{:S(2)}) %collective-permute-start.1) | collective-permute-done | bytes 524320 | tf_op jit(solution)/shard_map/ppermute | solution.py:104
  26.6 2.0 %collective-permute-start.4 = (bf16[128,1024]{1,0:T(8,128)(2,1)}, bf16[128,1024]{1,0:T(8,128)(2,1)}, u32[]{:S(2)}, u32[]{:S(2)}) collective-permute-start(bf16[128,1024]{1,0:T(8,128)(2,1)} %get-tuple-element.66), channel_id=1, source_target_pairs={{0,2},{1,3},{2,0},{3,1},{4,6},{5,7},{6,4},{7,5},{8,10},{9,11},{10,... | collective-permute-start | bytes 786440 | tf_op jit(solution)/shard_map/ppermute | solution.py:104
  28.6 1.7 %fusion.3 = f32[16,1536]{1,0:T(8,128)} fusion(f32[16,1536]{1,0:T(8,128)} %copy-done.14, f32[16,1536]{1,0:T(8,128)} %copy-done.13, f32[16,1536]{1,0:T(8,128)S(1)} %collective-permute-done.10, f32[4,16,1536]{2,1,0:T(8,128)} %copy-done.8, s32[]{:T(128)S(6)} %select_n.56), kind=kLoop, calls=%fused_computation.29 | loop fusion | flops 73728 | bytes 491524 | tf_op jit(solution)/shard_map/add | solution.py:332
  30.2 1.0 reshape.84
  31.2 0.6 copy-done.11
  31.9 1.7 %fusion.16 = (f32[2,4,768]{2,1,0:T(4,128)S(1)}, f32[2,1,4,768]{3,1,2,0:T(1,128)}, f32[2,4,768]{2,1,0:T(4,128)S(1)}) fusion(f32[2,1,4,768]{3,2,1,0:T(4,128)S(1)} %get-tuple-element.74, f32[4]{0:T(128)S(1)} %get-tuple-element.86, f32[2,4,4,768]{3,1,2,0:T(4,128)S(1)} %bitcast.74, f32[2,1,4,768]{3,2,1,0:T(4,128)} %get-tuple-element.75, f32[4]{0:T(128)S(1)} %get-tuple-element.85), kind=kLoop, calls=%fused_computation.71 | loop fusion | flops 122880 | bytes 172064 | tf_op jit(solution)/shard_map/add | solution.py:94
  33.7 4.5 %reduce-window.6 = f32[2,2,4,6,128]{4,3,2,1,0:T(8,128)S(1)} reduce-window(f32[2,2,4,6,128]{4,3,2,1,0:T(8,128)S(1)} %copy.72, f32[]{:T(128)} %constant.60.clone.1), window={size=1x1x1x1x128 pad=0_0x0_0x0_0x0_0x127_0}, to_apply=%region_0.1 | reduce-window | flops 1560576 | bytes 98308 | tf_op jit(solution)/shard_map/reduce-window
  38.4 0.7 reduce-window.9
  39.4 1.1 fusion.9
  40.7 14.5 %all-gather = f32[16,2,2,4]{3,2,1,0:T(2,128)S(1)} all-gather(f32[2,2,2,4]{3,2,1,0:T(2,128)S(1)} %pad_maximum_fusion.2), channel_id=2, replica_groups=mesh['sp'=8,'tp'=4] {'sp'}, dimensions={0}, use_global_device_ids=true | all-gather | bytes 1152 | tf_op jit(solution)/shard_map/all_gather | solution.py:337
  55.6 1.5 collective-permute-start.7
  57.3 0.6 collective-permute-start.9
  57.9 0.6 fusion.15
  58.6 1.5 collective-permute-start.6
  60.1 0.5 collective-permute-start.8
  60.8 2.2 %copy-done.1 = bf16[4096,512]{1,0:T(8,128)(2,1)S(1)} copy-done((bf16[4096,512]{1,0:T(8,128)(2,1)S(1)}, bf16[4096,512]{1,0:T(8,128)(2,1)}, u32[]{:S(2)}) %copy-start.1) | copy-done | bytes 4194328
  62.9 2.2 %copy-done.3 = bf16[4096,512]{1,0:T(8,128)(2,1)S(1)} copy-done((bf16[4096,512]{1,0:T(8,128)(2,1)S(1)}, bf16[4096,512]{1,0:T(8,128)(2,1)}, u32[]{:S(2)}) %copy-start.3) | copy-done | bytes 4194328
  65.1 1.9 %copy-done.6 = bf16[2,768,1024]{2,1,0:T(8,128)(2,1)S(1)} copy-done((bf16[2,768,1024]{2,1,0:T(8,128)(2,1)S(1)}, bf16[2,768,1024]{2,1,0:T(8,128)(2,1)}, u32[]{:S(2)}) %copy-start.6) | copy-done | bytes 3145752
  67.0 6.1 %early.2.acc = f32[4,768,256]{2,1,0:T(8,128)S(1)} custom-call(s32[5]{0:T(128)S(1)} %stack.40.feature, bf16[2,768,1024]{2,1,0:T(8,128)(2,1)S(1)} %copy-done.6, bf16[128,1024]{1,0:T(8,128)(2,1)S(1)} %collective-permute-done.refs_0_, bf16[256,1024]{1,0:T(8,128)(2,1)S(1)} %collective-permute-done.1.refs_1_, ...), custom_call_target="tpu_custom_call" | custom-call | tf_op jit(solution)/shard_map/early/pallas_call | solution.py:148
  73.2 2.3 %collective-permute-done.6.refs_0_ = bf16[128,1024]{1,0:T(8,128)(2,1)S(1)} collective-permute-done((bf16[128,1024]{1,0:T(8,128)(2,1)S(1)}, bf16[128,1024]{1,0:T(8,128)(2,1)S(1)}, u32[]{:S(2)}, u32[]{:S(2)}) %collective-permute-start.6) | collective-permute-done | bytes 262176 | tf_op jit(solution)/shard_map/ppermute | solution.py:104
  75.4 1.4 collective-permute-done.8.refs_2_
  76.9 4.9 %late.4 = (f32[4,136,128]{2,1,0:T(8,128)S(1)}, f32[4,136,128]{2,1,0:T(8,128)S(1)}) custom-call(s32[5]{0:T(128)S(1)} %stack.40.feature, f32[4,768,256]{2,1,0:T(8,128)S(1)} %early.2.acc, bf16[128,1024]{1,0:T(8,128)(2,1)S(1)} %collective-permute-done.6.refs_0_, bf16[256,1024]{1,0:T(8,128)(2,1)} %collective-permute-done.7.refs_1_, ...), custom_call_target="tpu_custom_call" | custom-call | tf_op jit(solution)/shard_map/late/pallas_call | solution.py:210
  82.0 0.6 collective-permute-start.21
  82.6 1.5 collective-permute-start.17
  84.1 0.5 collective-permute-start.20
  84.6 1.6 collective-permute-start.18
  86.2 0.5 collective-permute-start.19
  86.8 16.2 %collective-permute-done.18.refs_1_ = bf16[128,1024]{1,0:T(8,128)(2,1)S(1)} collective-permute-done((bf16[128,1024]{1,0:T(8,128)(2,1)S(1)}, bf16[128,1024]{1,0:T(8,128)(2,1)S(1)}, u32[]{:S(2)}, u32[]{:S(2)}) %collective-permute-start.18) | collective-permute-done | bytes 262176 | tf_op jit(solution)/shard_map/ppermute | solution.py:104
  103.0 1.6 collective-permute-start.14
  104.5 1.5 collective-permute-start.22
  106.6 1.5 collective-permute-done.14
  108.0 1.5 collective-permute-start.24
  109.6 9.7 %collective-permute-done.22.refs_5_ = bf16[128,1024]{1,0:T(8,128)(2,1)S(1)} collective-permute-done((bf16[128,1024]{1,0:T(8,128)(2,1)S(1)}, bf16[128,1024]{1,0:T(8,128)(2,1)S(1)}, u32[]{:S(2)}, u32[]{:S(2)}) %collective-permute-start.22) | collective-permute-done | bytes 262176 | tf_op jit(solution)/shard_map/ppermute | solution.py:104
  119.3 0.6 collective-permute-start.15
  120.4 7.5 %collective-permute-done.15 = bf16[4,136,128]{2,1,0:T(8,128)(2,1)S(1)} collective-permute-done((bf16[4,136,128]{2,1,0:T(8,128)(2,1)S(1)}, bf16[4,136,128]{2,1,0:T(8,128)(2,1)S(1)}, u32[]{:S(2)}, u32[]{:S(2)}) %collective-permute-start.15) | collective-permute-done | bytes 139296 | tf_op jit(solution)/shard_map/ppermute | solution.py:104
  127.9 0.5 collective-permute-start.23
  128.6 5.6 %early.3.acc = f32[4,768,256]{2,1,0:T(8,128)S(1)} custom-call(s32[5]{0:T(128)S(1)} %stack.40.feature, bf16[2,768,1024]{2,1,0:T(8,128)(2,1)S(1)} %copy-done.6, bf16[256,1024]{1,0:T(8,128)(2,1)S(1)} %collective-permute-done.17.refs_0_, bf16[128,1024]{1,0:T(8,128)(2,1)S(1)} %collective-permute-done.18.refs_1_, ...), custom_call_target="tpu_custom_call" | custom-call | tf_op jit(solution)/shard_map/early/pallas_call | solution.py:148
  134.2 3.3 %late.5.refs_5_ = f32[4,272,256]{2,1,0:T(8,128)S(1)} custom-call(s32[5]{0:T(128)S(1)} %stack.40.feature, f32[4,768,256]{2,1,0:T(8,128)S(1)} %early.3.acc, bf16[256,1024]{1,0:T(8,128)(2,1)S(1)} %collective-permute-done.24.refs_0_, bf16[256,1024]{1,0:T(8,128)(2,1)S(1)} %collective-permute-done.25.refs_1_, bf16[4096,512]{1,0:T(8,128)(2,1)S(1)} %copy-done.2, ...), custom_call_target="tpu_custom_call" | custom-call | tf_op jit(solution)/shard_map/late/pallas_call | solution.py:210
  137.6 1.6 %late.7 = (f32[2,136,128]{2,1,0:T(8,128)S(1)}, f32[2,136,128]{2,1,0:T(8,128)S(1)}) custom-call(s32[5]{0:T(128)S(1)} %stack.40.feature, f32[4,768,256]{2,1,0:T(8,128)S(1)} %early.3.acc, bf16[128,1024]{1,0:T(8,128)(2,1)S(1)} %collective-permute-done.23.refs_0_, bf16[128,1024]{1,0:T(8,128)(2,1)S(1)} %collective-permute-done.26.refs_1_, ...), custom_call_target="tpu_custom_call" | custom-call | tf_op jit(solution)/shard_map/late/pallas_call | solution.py:210
  139.2 0.6 collective-permute-start.31
  139.8 1.6 %late.6 = (f32[2,136,128]{2,1,0:T(8,128)S(1)}, f32[2,136,128]{2,1,0:T(8,128)S(1)}) custom-call(s32[5]{0:T(128)S(1)} %stack.40.feature, f32[4,768,256]{2,1,0:T(8,128)S(1)} %early.3.acc, bf16[128,1024]{1,0:T(8,128)(2,1)S(1)} %collective-permute-done.23.refs_0_, bf16[128,1024]{1,0:T(8,128)(2,1)S(1)} %collective-permute-done.26.refs_1_, ...), custom_call_target="tpu_custom_call" | custom-call | tf_op jit(solution)/shard_map/late/pallas_call | solution.py:210
  141.6 1.2 collective-permute-done.27
  142.8 0.9 collective-permute-start.28
  143.7 2.9 %collective-permute-done.32 = bf16[2,136,128]{2,1,0:T(8,128)(2,1)S(1)} collective-permute-done((bf16[2,136,128]{2,1,0:T(8,128)(2,1)S(1)}, bf16[2,136,128]{2,1,0:T(8,128)(2,1)S(1)}, u32[]{:S(2)}, u32[]{:S(2)}) %collective-permute-start.32) | collective-permute-done | bytes 69664 | tf_op jit(solution)/shard_map/ppermute | solution.py:104
  146.8 0.8 collective-permute-done.28
  147.6 2.1 %collective-permute-start.29 = (bf16[2,136,128]{2,1,0:T(8,128)(2,1)S(1)}, bf16[2,136,128]{2,1,0:T(8,128)(2,1)S(1)}, u32[]{:S(2)}, u32[]{:S(2)}) collective-permute-start(bf16[2,136,128]{2,1,0:T(8,128)(2,1)S(1)} %add_convert_fusion.7), channel_id=1, source_target_pairs={{0,16},{4,20},{8,24},{12,28},{16,0},{20,4},{24,8},{28,12},{1,17},{... | collective-permute-start | bytes 208904 | tf_op jit(solution)/shard_map/ppermute | solution.py:104
  149.7 4.4 %collective-permute-done.33 = bf16[2,136,128]{2,1,0:T(8,128)(2,1)S(1)} collective-permute-done((bf16[2,136,128]{2,1,0:T(8,128)(2,1)S(1)}, bf16[2,136,128]{2,1,0:T(8,128)(2,1)S(1)}, u32[]{:S(2)}, u32[]{:S(2)}) %collective-permute-start.33) | collective-permute-done | bytes 69664 | tf_op jit(solution)/shard_map/ppermute | solution.py:104
  154.2 1.1 collective-permute-done.29
  155.5 1.2 collective-permute-done.30.refs_3_
  156.6 1.2 read.1
  (103 shorter events, 4.8 us)
Async XLA Ops:
  0.6 1.0 copy-start
  1.9 7.8 %copy-start.5 = (bf16[2,768,1024]{2,1,0:T(8,128)(2,1)S(1)}, bf16[2,768,1024]{2,1,0:T(8,128)(2,1)}, u32[]{:S(2)}) copy-start(bf16[2,768,1024]{2,1,0:T(8,128)(2,1)} %own.3) | copy-start | bytes 9437188
  1.9 13.1 %copy-start.12 = (f32[2,4,4,768]{3,2,1,0:T(4,128)S(1)}, f32[2,4,4,768]{3,2,1,0:T(4,128)}, u32[]{:S(2)}) copy-start(f32[2,4,4,768]{3,2,1,0:T(4,128)} %param.12) | copy-start | bytes 294916
  2.0 13.7 %copy-start.15 = (f32[2,16]{1,0:T(2,128)S(1)}, f32[2,16]{1,0:T(2,128)}, u32[]{:S(2)}) copy-start(f32[2,16]{1,0:T(2,128)} %param.11) | copy-start | bytes 388
  5.1 8.4 %copy-start.8 = (f32[4,16,1536]{2,1,0:T(8,128)}, f32[4,16,1536]{2,1,0:T(8,128)S(1)}, u32[]{:S(2)}) copy-start(f32[4,16,1536]{2,1,0:T(8,128)S(1)} %fusion.21) | copy-start | bytes 1179652
  5.1 14.4 %collective-permute-start.10 = (f32[16,1536]{1,0:T(8,128)S(1)}, f32[16,1536]{1,0:T(8,128)S(1)}, u32[]{:S(2)}, u32[]{:S(2)}) collective-permute-start(f32[16,1536]{1,0:T(8,128)S(1)} %get-tuple-element.70), channel_id=1, source_target_pairs={{0,1},{1,0},{2,3},{3,2},{4,5},{5,4},{6,7},{7,6},{8,9},{9,8},{10,11... | collective-permute-start | bytes 294920 | tf_op jit(solution)/shard_map/ppermute | solution.py:104
  8.2 11.9 %collective-permute-start.11 = (f32[16,1536]{1,0:T(8,128)S(1)}, f32[16,1536]{1,0:T(8,128)S(1)}, u32[]{:S(2)}, u32[]{:S(2)}) collective-permute-start(f32[16,1536]{1,0:T(8,128)S(1)} %get-tuple-element.69), channel_id=1, source_target_pairs={{0,2},{1,3},{2,0},{3,1},{4,6},{5,7},{6,4},{7,5},{8,10},{9,11},{10,... | collective-permute-start | bytes 294920 | tf_op jit(solution)/shard_map/ppermute | solution.py:104
  9.7 12.5 %collective-permute-start.12 = (f32[16,1536]{1,0:T(8,128)S(1)}, f32[16,1536]{1,0:T(8,128)S(1)}, u32[]{:S(2)}, u32[]{:S(2)}) collective-permute-start(f32[16,1536]{1,0:T(8,128)S(1)} %get-tuple-element.68), channel_id=1, source_target_pairs={{0,3},{1,2},{2,1},{3,0},{4,7},{5,6},{6,5},{7,4},{8,11},{9,10},{10,... | collective-permute-start | bytes 294920 | tf_op jit(solution)/shard_map/ppermute | solution.py:104
  11.6 15.0 %collective-permute-start.1 = (bf16[256,1024]{1,0:T(8,128)(2,1)}, bf16[256,1024]{1,0:T(8,128)(2,1)S(1)}, u32[]{:S(2)}, u32[]{:S(2)}) collective-permute-start(bf16[256,1024]{1,0:T(8,128)(2,1)} %get-tuple-element.65), channel_id=1, source_target_pairs={{0,1},{1,0},{2,3},{3,2},{4,5},{5,4},{6,7},{7,6},{8,9},{9,8},{10,11... | collective-permute-start | bytes 1572872 | tf_op jit(solution)/shard_map/ppermute | solution.py:104
  13.5 15.0 %collective-permute-start.5 = (bf16[256,1024]{1,0:T(8,128)(2,1)}, bf16[256,1024]{1,0:T(8,128)(2,1)S(1)}, u32[]{:S(2)}, u32[]{:S(2)}) collective-permute-start(bf16[256,1024]{1,0:T(8,128)(2,1)} %get-tuple-element.64), channel_id=1, source_target_pairs={{0,2},{1,3},{2,0},{3,1},{4,6},{5,7},{6,4},{7,5},{8,10},{9,11},{10,... | collective-permute-start | bytes 1572872 | tf_op jit(solution)/shard_map/ppermute | solution.py:104
  19.5 37.8 %collective-permute-start = (bf16[128,1024]{1,0:T(8,128)(2,1)}, bf16[128,1024]{1,0:T(8,128)(2,1)S(1)}, u32[]{:S(2)}, u32[]{:S(2)}) collective-permute-start(bf16[128,1024]{1,0:T(8,128)(2,1)} %get-tuple-element.67), channel_id=1, source_target_pairs={{0,1},{1,0},{2,3},{3,2},{4,5},{5,4},{6,7},{7,6},{8,9},{9,8},{10,11... | collective-permute-start | bytes 786440 | tf_op jit(solution)/shard_map/ppermute | solution.py:104
  20.0 0.6 copy-start.13
  20.7 39.4 %collective-permute-start.2 = (bf16[384,1024]{1,0:T(8,128)(2,1)}, bf16[384,1024]{1,0:T(8,128)(2,1)S(1)}, u32[]{:S(2)}, u32[]{:S(2)}) collective-permute-start(bf16[384,1024]{1,0:T(8,128)(2,1)} %get-tuple-element.63), channel_id=1, source_target_pairs={{0,1},{1,0},{2,3},{3,2},{4,5},{5,4},{6,7},{7,6},{8,9},{9,8},{10,11... | collective-permute-start | bytes 2359304 | tf_op jit(solution)/shard_map/ppermute | solution.py:104
  22.2 0.7 copy-start.14
  22.8 37.9 %collective-permute-start.3 = (bf16[384,1024]{1,0:T(8,128)(2,1)}, bf16[384,1024]{1,0:T(8,128)(2,1)S(1)}, u32[]{:S(2)}, u32[]{:S(2)}) collective-permute-start(bf16[384,1024]{1,0:T(8,128)(2,1)} %get-tuple-element.62), channel_id=1, source_target_pairs={{0,2},{1,3},{2,0},{3,1},{4,6},{5,7},{6,4},{7,5},{8,10},{9,11},{10,... | collective-permute-start | bytes 2359304 | tf_op jit(solution)/shard_map/ppermute | solution.py:104
  26.6 32.0 %collective-permute-start.4 = (bf16[128,1024]{1,0:T(8,128)(2,1)}, bf16[128,1024]{1,0:T(8,128)(2,1)}, u32[]{:S(2)}, u32[]{:S(2)}) collective-permute-start(bf16[128,1024]{1,0:T(8,128)(2,1)} %get-tuple-element.66), channel_id=1, source_target_pairs={{0,2},{1,3},{2,0},{3,1},{4,6},{5,7},{6,4},{7,5},{8,10},{9,11},{10,... | collective-permute-start | bytes 786440 | tf_op jit(solution)/shard_map/ppermute | solution.py:104
  31.2 0.6 copy-start.11
  55.6 21.2 %collective-permute-start.7 = (bf16[256,1024]{1,0:T(8,128)(2,1)S(1)}, bf16[256,1024]{1,0:T(8,128)(2,1)}, u32[]{:S(2)}, u32[]{:S(2)}) collective-permute-start(bf16[256,1024]{1,0:T(8,128)(2,1)S(1)} %collective-permute-done.1.refs_1_), channel_id=1, source_target_pairs={{0,2},{1,3},{2,0},{3,1},{4,6},{5,7},{6,4},{7,5},{8,10},{9,11},{10,... | collective-permute-start | bytes 1572872 | tf_op jit(solution)/shard_map/ppermute | solution.py:104
  57.3 19.6 %collective-permute-start.9 = (bf16[256,1024]{1,0:T(8,128)(2,1)S(1)}, bf16[256,1024]{1,0:T(8,128)(2,1)}, u32[]{:S(2)}, u32[]{:S(2)}) collective-permute-start(bf16[256,1024]{1,0:T(8,128)(2,1)S(1)} %collective-permute-done.5.refs_5_), channel_id=1, source_target_pairs={{0,1},{1,0},{2,3},{3,2},{4,5},{5,4},{6,7},{7,6},{8,9},{9,8},{10,11... | collective-permute-start | bytes 1572872 | tf_op jit(solution)/shard_map/ppermute | solution.py:104
  58.6 16.9 %collective-permute-start.6 = (bf16[128,1024]{1,0:T(8,128)(2,1)S(1)}, bf16[128,1024]{1,0:T(8,128)(2,1)S(1)}, u32[]{:S(2)}, u32[]{:S(2)}) collective-permute-start(bf16[128,1024]{1,0:T(8,128)(2,1)S(1)} %collective-permute-done.refs_0_), channel_id=1, source_target_pairs={{0,2},{1,3},{2,0},{3,1},{4,6},{5,7},{6,4},{7,5},{8,10},{9,11},{10,... | collective-permute-start | bytes 786440 | tf_op jit(solution)/shard_map/ppermute | solution.py:104
  60.1 16.8 %collective-permute-start.8 = (bf16[128,1024]{1,0:T(8,128)(2,1)}, bf16[128,1024]{1,0:T(8,128)(2,1)S(1)}, u32[]{:S(2)}, u32[]{:S(2)}) collective-permute-start(bf16[128,1024]{1,0:T(8,128)(2,1)} %collective-permute-done.4.refs_4_), channel_id=1, source_target_pairs={{0,1},{1,0},{2,3},{3,2},{4,5},{5,4},{6,7},{7,6},{8,9},{9,8},{10,11... | collective-permute-start | bytes 786440 | tf_op jit(solution)/shard_map/ppermute | solution.py:104
  60.7 2.2 %copy-start.1 = (bf16[4096,512]{1,0:T(8,128)(2,1)S(1)}, bf16[4096,512]{1,0:T(8,128)(2,1)}, u32[]{:S(2)}) copy-start(bf16[4096,512]{1,0:T(8,128)(2,1)} %refs_2_.5) | copy-start | bytes 12582916
  62.9 2.2 %copy-start.3 = (bf16[4096,512]{1,0:T(8,128)(2,1)S(1)}, bf16[4096,512]{1,0:T(8,128)(2,1)}, u32[]{:S(2)}) copy-start(bf16[4096,512]{1,0:T(8,128)(2,1)} %refs_3_.5) | copy-start | bytes 12582916
  65.1 1.9 %copy-start.6 = (bf16[2,768,1024]{2,1,0:T(8,128)(2,1)S(1)}, bf16[2,768,1024]{2,1,0:T(8,128)(2,1)}, u32[]{:S(2)}) copy-start(bf16[2,768,1024]{2,1,0:T(8,128)(2,1)} %own.3) | copy-start | bytes 9437188
  67.0 9.9 %copy-start.2 = (bf16[4096,512]{1,0:T(8,128)(2,1)S(1)}, bf16[4096,512]{1,0:T(8,128)(2,1)}, u32[]{:S(2)}) copy-start(bf16[4096,512]{1,0:T(8,128)(2,1)} %refs_2_.5) | copy-start | bytes 12582916
  67.0 9.9 %copy-start.4 = (bf16[4096,512]{1,0:T(8,128)(2,1)S(1)}, bf16[4096,512]{1,0:T(8,128)(2,1)}, u32[]{:S(2)}) copy-start(bf16[4096,512]{1,0:T(8,128)(2,1)} %refs_3_.5) | copy-start | bytes 12582916
  76.9 7.2 %copy-start.10 = (bf16[384,1024]{1,0:T(8,128)(2,1)S(1)}, bf16[384,1024]{1,0:T(8,128)(2,1)}, u32[]{:S(2)}) copy-start(bf16[384,1024]{1,0:T(8,128)(2,1)} %get-tuple-element.60) | copy-start | bytes 2359300
  81.8 4.4 %copy-start.9 = (bf16[384,1024]{1,0:T(8,128)(2,1)S(1)}, bf16[384,1024]{1,0:T(8,128)(2,1)}, u32[]{:S(2)}) copy-start(bf16[384,1024]{1,0:T(8,128)(2,1)} %get-tuple-element.61) | copy-start | bytes 2359300
  81.8 4.4 %collective-permute-start.13 = (f32[4,136,128]{2,1,0:T(8,128)S(1)}, f32[4,136,128]{2,1,0:T(8,128)S(1)}, u32[]{:S(2)}, u32[]{:S(2)}) collective-permute-start(f32[4,136,128]{2,1,0:T(8,128)S(1)} %get-tuple-element.34), channel_id=1, source_target_pairs={{0,4},{4,0},{8,12},{12,8},{16,20},{20,16},{24,28},{28,24},{1,5},{5... | collective-permute-start | bytes 835592 | tf_op jit(solution)/shard_map/ppermute | solution.py:104
  82.0 22.6 %collective-permute-start.21 = (bf16[256,1024]{1,0:T(8,128)(2,1)S(1)}, bf16[256,1024]{1,0:T(8,128)(2,1)S(1)}, u32[]{:S(2)}, u32[]{:S(2)}) collective-permute-start(bf16[256,1024]{1,0:T(8,128)(2,1)S(1)} %get-tuple-element.58), channel_id=1, source_target_pairs={{0,2},{1,3},{2,0},{3,1},{4,6},{5,7},{6,4},{7,5},{8,10},{9,11},{10,... | collective-permute-start | bytes 1572872 | tf_op jit(solution)/shard_map/ppermute | solution.py:104
  82.6 23.5 %collective-permute-start.17 = (bf16[256,1024]{1,0:T(8,128)(2,1)S(1)}, bf16[256,1024]{1,0:T(8,128)(2,1)S(1)}, u32[]{:S(2)}, u32[]{:S(2)}) collective-permute-start(bf16[256,1024]{1,0:T(8,128)(2,1)S(1)} %get-tuple-element.59), channel_id=1, source_target_pairs={{0,1},{1,0},{2,3},{3,2},{4,5},{5,4},{6,7},{7,6},{8,9},{9,8},{10,11... | collective-permute-start | bytes 1572872 | tf_op jit(solution)/shard_map/ppermute | solution.py:104
  84.1 35.8 %collective-permute-start.20 = (bf16[384,1024]{1,0:T(8,128)(2,1)S(1)}, bf16[384,1024]{1,0:T(8,128)(2,1)S(1)}, u32[]{:S(2)}, u32[]{:S(2)}) collective-permute-start(bf16[384,1024]{1,0:T(8,128)(2,1)S(1)} %copy-done.10), channel_id=1, source_target_pairs={{0,2},{1,3},{2,0},{3,1},{4,6},{5,7},{6,4},{7,5},{8,10},{9,11},{10,... | collective-permute-start | bytes 2359304 | tf_op jit(solution)/shard_map/ppermute | solution.py:104
  84.6 18.3 %collective-permute-start.18 = (bf16[128,1024]{1,0:T(8,128)(2,1)S(1)}, bf16[128,1024]{1,0:T(8,128)(2,1)S(1)}, u32[]{:S(2)}, u32[]{:S(2)}) collective-permute-start(bf16[128,1024]{1,0:T(8,128)(2,1)S(1)} %get-tuple-element.57), channel_id=1, source_target_pairs={{0,1},{1,0},{2,3},{3,2},{4,5},{5,4},{6,7},{7,6},{8,9},{9,8},{10,11... | collective-permute-start | bytes 786440 | tf_op jit(solution)/shard_map/ppermute | solution.py:104
  86.2 42.3 %collective-permute-start.19 = (bf16[384,1024]{1,0:T(8,128)(2,1)S(1)}, bf16[384,1024]{1,0:T(8,128)(2,1)S(1)}, u32[]{:S(2)}, u32[]{:S(2)}) collective-permute-start(bf16[384,1024]{1,0:T(8,128)(2,1)S(1)} %copy-done.9), channel_id=1, source_target_pairs={{0,1},{1,0},{2,3},{3,2},{4,5},{5,4},{6,7},{7,6},{8,9},{9,8},{10,11... | collective-permute-start | bytes 2359304 | tf_op jit(solution)/shard_map/ppermute | solution.py:104
  103.0 5.1 %collective-permute-start.14 = (bf16[4,136,128]{2,1,0:T(8,128)(2,1)S(1)}, bf16[4,136,128]{2,1,0:T(8,128)(2,1)S(1)}, u32[]{:S(2)}, u32[]{:S(2)}) collective-permute-start(bf16[4,136,128]{2,1,0:T(8,128)(2,1)S(1)} %add_convert_fusion.2), channel_id=1, source_target_pairs={{0,8},{4,12},{8,0},{12,4},{16,24},{20,28},{24,16},{28,20},{1,9},{5... | collective-permute-start | bytes 417800 | tf_op jit(solution)/shard_map/ppermute | solution.py:104
  104.5 14.8 %collective-permute-start.22 = (bf16[128,1024]{1,0:T(8,128)(2,1)S(1)}, bf16[128,1024]{1,0:T(8,128)(2,1)S(1)}, u32[]{:S(2)}, u32[]{:S(2)}) collective-permute-start(bf16[128,1024]{1,0:T(8,128)(2,1)S(1)} %get-tuple-element.56), channel_id=1, source_target_pairs={{0,2},{1,3},{2,0},{3,1},{4,6},{5,7},{6,4},{7,5},{8,10},{9,11},{10,... | collective-permute-start | bytes 786440 | tf_op jit(solution)/shard_map/ppermute | solution.py:104
  106.0 28.2 %collective-permute-start.25 = (bf16[256,1024]{1,0:T(8,128)(2,1)S(1)}, bf16[256,1024]{1,0:T(8,128)(2,1)S(1)}, u32[]{:S(2)}, u32[]{:S(2)}) collective-permute-start(bf16[256,1024]{1,0:T(8,128)(2,1)S(1)} %collective-permute-done.21.refs_4_), channel_id=1, source_target_pairs={{0,1},{1,0},{2,3},{3,2},{4,5},{5,4},{6,7},{7,6},{8,9},{9,8},{10,11... | collective-permute-start | bytes 1572872 | tf_op jit(solution)/shard_map/ppermute | solution.py:104
  108.0 26.2 %collective-permute-start.24 = (bf16[256,1024]{1,0:T(8,128)(2,1)S(1)}, bf16[256,1024]{1,0:T(8,128)(2,1)S(1)}, u32[]{:S(2)}, u32[]{:S(2)}) collective-permute-start(bf16[256,1024]{1,0:T(8,128)(2,1)S(1)} %collective-permute-done.17.refs_0_), channel_id=1, source_target_pairs={{0,2},{1,3},{2,0},{3,1},{4,6},{5,7},{6,4},{7,5},{8,10},{9,11},{10,... | collective-permute-start | bytes 1572872 | tf_op jit(solution)/shard_map/ppermute | solution.py:104
  119.3 8.6 %collective-permute-start.15 = (bf16[4,136,128]{2,1,0:T(8,128)(2,1)S(1)}, bf16[4,136,128]{2,1,0:T(8,128)(2,1)S(1)}, u32[]{:S(2)}, u32[]{:S(2)}) collective-permute-start(bf16[4,136,128]{2,1,0:T(8,128)(2,1)S(1)} %add_convert_fusion.1), channel_id=1, source_target_pairs={{0,16},{4,20},{8,24},{12,28},{16,0},{20,4},{24,8},{28,12},{1,17},{... | collective-permute-start | bytes 417800 | tf_op jit(solution)/shard_map/ppermute | solution.py:104
  119.9 17.7 %collective-permute-start.26 = (bf16[128,1024]{1,0:T(8,128)(2,1)S(1)}, bf16[128,1024]{1,0:T(8,128)(2,1)S(1)}, u32[]{:S(2)}, u32[]{:S(2)}) collective-permute-start(bf16[128,1024]{1,0:T(8,128)(2,1)S(1)} %collective-permute-done.22.refs_5_), channel_id=1, source_target_pairs={{0,1},{1,0},{2,3},{3,2},{4,5},{5,4},{6,7},{7,6},{8,9},{9,8},{10,11... | collective-permute-start | bytes 786440 | tf_op jit(solution)/shard_map/ppermute | solution.py:104
  127.9 9.7 %collective-permute-start.23 = (bf16[128,1024]{1,0:T(8,128)(2,1)S(1)}, bf16[128,1024]{1,0:T(8,128)(2,1)S(1)}, u32[]{:S(2)}, u32[]{:S(2)}) collective-permute-start(bf16[128,1024]{1,0:T(8,128)(2,1)S(1)} %collective-permute-done.18.refs_1_), channel_id=1, source_target_pairs={{0,2},{1,3},{2,0},{3,1},{4,6},{5,7},{6,4},{7,5},{8,10},{9,11},{10,... | collective-permute-start | bytes 786440 | tf_op jit(solution)/shard_map/ppermute | solution.py:104
  128.5 5.7 %collective-permute-start.16 = (bf16[4,136,128]{2,1,0:T(8,128)(2,1)S(1)}, bf16[4,136,128]{2,1,0:T(8,128)(2,1)S(1)}, u32[]{:S(2)}, u32[]{:S(2)}) collective-permute-start(bf16[4,136,128]{2,1,0:T(8,128)(2,1)S(1)} %add_convert_fusion.refs_0_), channel_id=1, source_target_pairs={{0,4},{4,0},{8,12},{12,8},{16,20},{20,16},{24,28},{28,24},{1,5},{5... | collective-permute-start | bytes 417800 | tf_op jit(solution)/shard_map/ppermute | solution.py:104
  139.2 17.4 %copy-start.7 = (bf16[2,128,512]{2,1,0:T(8,128)(2,1)S(1)}, bf16[2,128,512]{2,1,0:T(8,128)(2,1)}, u32[]{:S(2)}) copy-start(bf16[2,128,512]{2,1,0:T(8,128)(2,1)} %refs_6_.5) | copy-start | bytes 786436
  139.2 2.2 %collective-permute-start.31 = (f32[2,136,128]{2,1,0:T(8,128)S(1)}, f32[2,136,128]{2,1,0:T(8,128)S(1)}, u32[]{:S(2)}, u32[]{:S(2)}) collective-permute-start(f32[2,136,128]{2,1,0:T(8,128)S(1)} %get-tuple-element.48), channel_id=1, source_target_pairs={{0,4},{4,0},{8,12},{12,8},{16,20},{20,16},{24,28},{28,24},{1,5},{5... | collective-permute-start | bytes 417800 | tf_op jit(solution)/shard_map/ppermute | solution.py:104
  141.4 1.4 collective-permute-start.27
  141.5 5.1 %collective-permute-start.32 = (bf16[2,136,128]{2,1,0:T(8,128)(2,1)S(1)}, bf16[2,136,128]{2,1,0:T(8,128)(2,1)S(1)}, u32[]{:S(2)}, u32[]{:S(2)}) collective-permute-start(bf16[2,136,128]{2,1,0:T(8,128)(2,1)S(1)} %add_convert_fusion.5), channel_id=1, source_target_pairs={{0,8},{4,12},{8,0},{12,4},{16,24},{20,28},{24,16},{28,20},{1,9},{5... | collective-permute-start | bytes 208904 | tf_op jit(solution)/shard_map/ppermute | solution.py:104
  142.8 4.8 %collective-permute-start.28 = (bf16[2,136,128]{2,1,0:T(8,128)(2,1)S(1)}, bf16[2,136,128]{2,1,0:T(8,128)(2,1)S(1)}, u32[]{:S(2)}, u32[]{:S(2)}) collective-permute-start(bf16[2,136,128]{2,1,0:T(8,128)(2,1)S(1)} %add_convert_fusion.8), channel_id=1, source_target_pairs={{0,8},{4,12},{8,0},{12,4},{16,24},{20,28},{24,16},{28,20},{1,9},{5... | collective-permute-start | bytes 208904 | tf_op jit(solution)/shard_map/ppermute | solution.py:104
  146.6 7.5 %collective-permute-start.33 = (bf16[2,136,128]{2,1,0:T(8,128)(2,1)S(1)}, bf16[2,136,128]{2,1,0:T(8,128)(2,1)S(1)}, u32[]{:S(2)}, u32[]{:S(2)}) collective-permute-start(bf16[2,136,128]{2,1,0:T(8,128)(2,1)S(1)} %add_convert_fusion.4), channel_id=1, source_target_pairs={{0,16},{4,20},{8,24},{12,28},{16,0},{20,4},{24,8},{28,12},{1,17},{... | collective-permute-start | bytes 208904 | tf_op jit(solution)/shard_map/ppermute | solution.py:104
  147.6 7.7 %collective-permute-start.29 = (bf16[2,136,128]{2,1,0:T(8,128)(2,1)S(1)}, bf16[2,136,128]{2,1,0:T(8,128)(2,1)S(1)}, u32[]{:S(2)}, u32[]{:S(2)}) collective-permute-start(bf16[2,136,128]{2,1,0:T(8,128)(2,1)S(1)} %add_convert_fusion.7), channel_id=1, source_target_pairs={{0,16},{4,20},{8,24},{12,28},{16,0},{20,4},{24,8},{28,12},{1,17},{... | collective-permute-start | bytes 208904 | tf_op jit(solution)/shard_map/ppermute | solution.py:104
  154.1 1.3 collective-permute-start.34
  155.3 1.3 collective-permute-start.30
